TPU v7x, 32 devices: a whole 2x2x4 slice. The times are simulated.
32 devices in a mesh: sp: 8 (over z, y), tp: 4 (over x, core).
Axes of the slice: x: 2, y: 2, z: 4, core: 2. Of those that a mesh axis runs over, the one named last changes fastest.
Arguments:
- inputs: bfloat16 [8192, 2048], P(('sp', 'tp')), may hold values from -90 to 90
- in_gain: float32 [2048], replicated, may hold values from 0.1 to 1.9
- w_query: bfloat16 [2048, 1024], replicated, may hold values from -2 to 2
- w_key: bfloat16 [2048, 128], replicated, may hold values from -2 to 2
- w_value: bfloat16 [2048, 128], replicated, may hold values from -0.125 to 0.125
- query_gain: float32 [64], replicated, may hold values from 0 to 8, as said below
- key_gain: float32 [64], replicated, may hold values from 0 to 8, as said below
- decay_sums: float32 [8192, 16], P('sp', 'tp'), may hold values from -1173 to 0, as said below
- w_out: bfloat16 [1024, 2048], replicated, may hold values from -0.1875 to 0.1875
Outputs:
- result: bfloat16 [8192, 2048], P(('sp', 'tp'))
Inputs may be any that keep to these rules, and one draw needn't show every extreme that they name: `decay_sums`: along positions, each head's entries never rise. `query_gain`: every entry is positive. `key_gain`: every entry is positive.
All inputs are finite; a program needn't handle non-finite values.
Results may differ from a plain program's by a relative error of at most 0.015.
The roundings to bfloat16 on the way count: a program that leaves them out, or rounds other values in their place, can miss the bound.
Values may be sent and summed in bfloat16 or wider, within the bound.
A program may use at most 64 MiB of HBM per device.

v0:
```python
from functools import partial
import math

import jax
import jax.numpy as jnp
from jax import lax
from jax.sharding import PartitionSpec as P

epsilon = 1e-06


def rms_norm(vector, gain_vec):
    return (
        vector * lax.rsqrt(jnp.mean(vector * vector, axis=-1, keepdims=True) + epsilon) * gain_vec
    )


def attend_step(
    masked, query_rows, query_decay, query_pos, key_slice, value_slice, decay_slice, key_pos, inner
):
    peak, total, weighted = inner
    score_scale = query_rows.shape[2] ** (-0.5)
    scores = (
        jnp.einsum("thd,ud->htu", query_rows, key_slice, preferred_element_type=jnp.float32)
        * score_scale
    )
    scores = scores + query_decay[:, :, None] - decay_slice[:, None, :]
    if masked:
        visible = key_pos[None, :] <= query_pos[:, None]
        scores = jnp.where(visible[None], scores, -1e30)
    peak_new = jnp.maximum(peak, jnp.max(scores, axis=-1))
    weights_exp = jnp.exp(scores - peak_new[:, :, None])
    if masked:
        weights_exp = jnp.where(visible[None], weights_exp, 0.0)
    rescale = jnp.exp(peak - peak_new)
    total_new = total * rescale + jnp.sum(weights_exp, axis=-1)
    product = jnp.einsum(
        "htu,ud->thd",
        weights_exp.astype(jnp.bfloat16),
        value_slice,
        preferred_element_type=jnp.float32,
    )
    weighted_new = weighted * rescale.T[:, :, None] + product
    return (peak_new, total_new, weighted_new)


def keep_state(inner):
    return inner


def per_device(inputs, in_gain, w_query, w_key, w_value, query_gain, key_gain, decay_sums, w_out):
    tp_count = lax.axis_size("tp")
    sp_rank = lax.axis_index("sp")
    heads_dev = decay_sums.shape[1]
    head_size = query_gain.shape[0]
    kv_heads = w_key.shape[1] // head_size
    width_dev = heads_dev * head_size
    normed = rms_norm(inputs.astype(jnp.float32), in_gain).astype(jnp.bfloat16)
    row_count = normed.shape[0]
    all_heads = w_query.shape[1] // head_size
    query_all = rms_norm(
        jnp.dot(normed, w_query, preferred_element_type=jnp.float32).reshape(
            row_count, all_heads, head_size
        ),
        query_gain,
    ).astype(jnp.bfloat16)
    key_all = rms_norm(
        jnp.dot(normed, w_key, preferred_element_type=jnp.float32).reshape(
            row_count, kv_heads, head_size
        ),
        key_gain,
    ).astype(jnp.bfloat16)
    value_all = (
        jnp.dot(normed, w_value, preferred_element_type=jnp.float32)
        .astype(jnp.bfloat16)
        .reshape(row_count, kv_heads, head_size)
    )
    pair_all = jnp.repeat(
        jnp.concatenate([key_all, value_all], axis=2), tp_count // kv_heads, axis=1
    )
    packed = jnp.concatenate([query_all.reshape(row_count, tp_count, width_dev), pair_all], axis=2)
    received = lax.all_to_all(packed, "tp", split_axis=1, concat_axis=0, tiled=True)[:, 0]
    tok_rows = received.shape[0]
    queries = received[:, :width_dev].reshape(tok_rows, heads_dev, head_size)
    key_values = received[:, width_dev:]
    all_decays = lax.all_gather(decay_sums, "sp", axis=0, tiled=True)
    groups = (queries, sp_rank * tok_rows)
    prepared = []
    query_rows, first_pos = groups
    rows = query_rows.shape[0]
    query_decay = lax.dynamic_slice_in_dim(all_decays, first_pos, rows, 0).T
    query_pos = first_pos + jnp.arange(rows, dtype=jnp.int32)
    prepared.append((query_rows, query_decay, query_pos, first_pos, first_pos + rows - 1))
    initial = tuple(
        (
            (
                jnp.full((heads_dev, entry[0].shape[0]), -1e30, jnp.float32),
                jnp.zeros((heads_dev, entry[0].shape[0]), jnp.float32),
                jnp.zeros((entry[0].shape[0], heads_dev, head_size), jnp.float32),
            )
            for entry in prepared
        )
    )
    state = initial
    pieces = lax.all_gather(key_values, "sp", axis=0, tiled=True)
    piece_rows = pieces.shape[0]
    key_block = math.gcd(piece_rows, 512)

    def one_block(carry, block_index):
        key_start = block_index * key_block
        pair_slice = lax.dynamic_slice_in_dim(pieces, block_index * key_block, key_block, 0)
        key_slice = pair_slice[:, :head_size]
        value_slice = pair_slice[:, head_size:]
        decay_slice = lax.dynamic_slice_in_dim(all_decays, key_start, key_block, 0).T
        key_pos = key_start + jnp.arange(key_block, dtype=jnp.int32)
        updated = []
        for (query_rows, query_decay, query_pos, first_pos, last_pos), inner in zip(
            prepared, carry
        ):
            branch = jnp.where(
                key_start > last_pos, 0, jnp.where(key_start + key_block - 1 <= first_pos, 1, 2)
            )
            full_step = partial(
                attend_step,
                False,
                query_rows,
                query_decay,
                query_pos,
                key_slice,
                value_slice,
                decay_slice,
                key_pos,
            )
            masked_step = partial(
                attend_step,
                True,
                query_rows,
                query_decay,
                query_pos,
                key_slice,
                value_slice,
                decay_slice,
                key_pos,
            )
            updated.append(lax.switch(branch, [keep_state, full_step, masked_step], inner))
        return (tuple(updated), None)

    state, unused = lax.scan(one_block, state, jnp.arange(piece_rows // key_block, dtype=jnp.int32))
    outputs = [
        (weighted / total.T[:, :, None]).astype(jnp.bfloat16) for peak, total, weighted in state
    ]
    attended = outputs[0].reshape(tok_rows, width_dev)
    out_rows = lax.all_to_all(attended, "tp", split_axis=0, concat_axis=1, tiled=True)
    result = jnp.dot(out_rows, w_out, preferred_element_type=jnp.float32).astype(jnp.bfloat16)
    return result


def solution(mesh):
    placed = (P(("sp", "tp"), None), P(), P(), P(), P(), P(), P(), P("sp", "tp"), P())
    return jax.shard_map(
        per_device, mesh=mesh, in_specs=placed, out_specs=P(("sp", "tp"), None), check_vma=False
    )
```

profile of v0, /device:TPU:28, one launch (start us, length us, event | category | flops | bytes accessed | tf_op | source)
XLA Modules:
  0.0 254.3 jit_solution(247003745765237062)
XLA Ops:
  11.9 4.8 %fusion.51 = (f32[256,1024]{1,0:T(8,128)}, f32[256,1024]{1,0:T(8,128)S(1)}) fusion(bf16[2048,1024]{1,0:T(8,128)(2,1)} %param.16, bf16[256,2048]{1,0:T(8,128)(2,1)} %param.14, f32[2048]{0:T(1024)} %param.15, f32[256]{0:T(256)S(1)} %add_rsqrt_fusion.2), kind=kOutput, calls=%fused_computation.65 | convolution fusion | flops 1076101120 | bytes 7349248 | tf_op jit(solution)/shard_map/dot_general | solution.py:62
  19.3 14.2 %all_to_all.34 = bf16[256,4,384]{0,2,1:T(8,128)(2,1)S(1)} all-to-all(bf16[256,4,384]{0,2,1:T(8,128)(2,1)S(1)} %pad_maximum_fusion), channel_id=1, replica_groups=mesh['sp'=8,'tp'=4] {'tp'}, dimensions={1} | all-to-all | bytes 1572864 | tf_op jit(solution)/shard_map/all_to_all | solution.py:82
  34.6 31.2 %all_gather.7 = f32[8192,4]{0,1:T(4,128)S(1)} all-gather(f32[1024,4]{0,1:T(4,128)S(1)} %copy-done.1), channel_id=1, replica_groups=mesh['sp'=8,'tp'=4] {'sp'}, dimensions={0}, use_global_device_ids=true | all-gather | bytes 147456 | tf_op jit(solution)/shard_map/all_gather | solution.py:86
  66.1 15.7 %all-gather.2.cloned.1.call-done = bf16[8192,128]{1,0:T(8,128)(2,1)} async-done(((bf16[1024,128]{1,0:T(8,128)(2,1)}), bf16[8192,128]{1,0:T(8,128)(2,1)}) %all-gather.2.cloned.1.call-update) | async-done | bytes 2097168 | tf_op jit(solution)/shard_map/all_gather | solution.py:105
  81.9 149.1 %while.20 = (s32[]{:T(128)}, f32[4,1024]{1,0:T(4,128)S(1)}, f32[4,1024]{1,0:T(4,128)S(1)}, f32[1024,4,64]{0,2,1:T(8,128)S(1)}, s32[16]{0:T(128)S(1)}, /*index=5*...) while((s32[]{:T(128)}, f32[4,1024]{1,0:T(4,128)S(1)}, ...), condition=%wide.region_11.12_spmd.clone.clone, body=%wide.region_3.11_spmd.clone.clone.sunk | while | flops 577779200 | bytes 30917152 | solution.py:148
  84.5 6.3 %conditional.4 = ((f32[4,1024]{1,0:T(4,128)S(1)}, f32[4,1024]{1,0:T(4,128)S(1)}, f32[1024,4,64]{0,2,1:T(8,128)S(1)})) conditional(s32[]{:T(128)} %clamp.12, (f32[4,1024]{1,0:T(4,128)S(1)}, f32[4,1024]{1,0:T(4,128)S(1)}, f32[1024,4,64]{0,2,1:T(8,128)S(1)}) %tuple.72, (bf16[512,64]{0,1:T(8,128)(2,1)S(1)}, ...), branch_computations={%region_4.4_spmd, %region_5.7_spmd, %region_8.10_spmd} | conditional | flops 577779200 | bytes 30369832 | solution.py:145
  86.1 2.6 %fusion.11 = f32[1024,4,64]{0,2,1:T(8,128)S(1)} fusion(f32[512,1024,4]{1,0,2:T(8,128)S(1)} %get-tuple-element.449, f32[4,1024]{1,0:T(4,128)S(1)} %get-tuple-element.538, f32[4,512]{1,0:T(4,128)S(1)} %get-tuple-element.292, f32[4,1024]{1,0:T(4,128)S(1)} %get-tuple-element.291, f32[1024,4,64]{0,2,1:T(8,128)S(1)} %get-tuple-element.294, ...), kind=kOutput, calls=%fused_computation.9 | convolution fusion | flops 279445504 | bytes 10608640 | tf_op jit(solution)/shard_map/while/body/eval_jaxpr/cond/branch_1_fun/htu,ud->thd/dot_general | solution.py:37
  93.5 6.3 %conditional.4 = ((f32[4,1024]{1,0:T(4,128)S(1)}, f32[4,1024]{1,0:T(4,128)S(1)}, f32[1024,4,64]{0,2,1:T(8,128)S(1)})) conditional(s32[]{:T(128)} %clamp.12, (f32[4,1024]{1,0:T(4,128)S(1)}, f32[4,1024]{1,0:T(4,128)S(1)}, f32[1024,4,64]{0,2,1:T(8,128)S(1)}) %tuple.72, (bf16[512,64]{0,1:T(8,128)(2,1)S(1)}, ...), branch_computations={%region_4.4_spmd, %region_5.7_spmd, %region_8.10_spmd} | conditional | flops 577779200 | bytes 30369832 | solution.py:145
  95.1 2.6 %fusion.11 = f32[1024,4,64]{0,2,1:T(8,128)S(1)} fusion(f32[512,1024,4]{1,0,2:T(8,128)S(1)} %get-tuple-element.449, f32[4,1024]{1,0:T(4,128)S(1)} %get-tuple-element.538, f32[4,512]{1,0:T(4,128)S(1)} %get-tuple-element.292, f32[4,1024]{1,0:T(4,128)S(1)} %get-tuple-element.291, f32[1024,4,64]{0,2,1:T(8,128)S(1)} %get-tuple-element.294, ...), kind=kOutput, calls=%fused_computation.9 | convolution fusion | flops 279445504 | bytes 10608640 | tf_op jit(solution)/shard_map/while/body/eval_jaxpr/cond/branch_1_fun/htu,ud->thd/dot_general | solution.py:37
  102.5 6.3 %conditional.4 = ((f32[4,1024]{1,0:T(4,128)S(1)}, f32[4,1024]{1,0:T(4,128)S(1)}, f32[1024,4,64]{0,2,1:T(8,128)S(1)})) conditional(s32[]{:T(128)} %clamp.12, (f32[4,1024]{1,0:T(4,128)S(1)}, f32[4,1024]{1,0:T(4,128)S(1)}, f32[1024,4,64]{0,2,1:T(8,128)S(1)}) %tuple.72, (bf16[512,64]{0,1:T(8,128)(2,1)S(1)}, ...), branch_computations={%region_4.4_spmd, %region_5.7_spmd, %region_8.10_spmd} | conditional | flops 577779200 | bytes 30369832 | solution.py:145
  104.1 2.6 %fusion.11 = f32[1024,4,64]{0,2,1:T(8,128)S(1)} fusion(f32[512,1024,4]{1,0,2:T(8,128)S(1)} %get-tuple-element.449, f32[4,1024]{1,0:T(4,128)S(1)} %get-tuple-element.538, f32[4,512]{1,0:T(4,128)S(1)} %get-tuple-element.292, f32[4,1024]{1,0:T(4,128)S(1)} %get-tuple-element.291, f32[1024,4,64]{0,2,1:T(8,128)S(1)} %get-tuple-element.294, ...), kind=kOutput, calls=%fused_computation.9 | convolution fusion | flops 279445504 | bytes 10608640 | tf_op jit(solution)/shard_map/while/body/eval_jaxpr/cond/branch_1_fun/htu,ud->thd/dot_general | solution.py:37
  106.7 2.1 fusion.4
  111.5 6.3 %conditional.4 = ((f32[4,1024]{1,0:T(4,128)S(1)}, f32[4,1024]{1,0:T(4,128)S(1)}, f32[1024,4,64]{0,2,1:T(8,128)S(1)})) conditional(s32[]{:T(128)} %clamp.12, (f32[4,1024]{1,0:T(4,128)S(1)}, f32[4,1024]{1,0:T(4,128)S(1)}, f32[1024,4,64]{0,2,1:T(8,128)S(1)}) %tuple.72, (bf16[512,64]{0,1:T(8,128)(2,1)S(1)}, ...), branch_computations={%region_4.4_spmd, %region_5.7_spmd, %region_8.10_spmd} | conditional | flops 577779200 | bytes 30369832 | solution.py:145
  113.1 2.6 %fusion.11 = f32[1024,4,64]{0,2,1:T(8,128)S(1)} fusion(f32[512,1024,4]{1,0,2:T(8,128)S(1)} %get-tuple-element.449, f32[4,1024]{1,0:T(4,128)S(1)} %get-tuple-element.538, f32[4,512]{1,0:T(4,128)S(1)} %get-tuple-element.292, f32[4,1024]{1,0:T(4,128)S(1)} %get-tuple-element.291, f32[1024,4,64]{0,2,1:T(8,128)S(1)} %get-tuple-element.294, ...), kind=kOutput, calls=%fused_computation.9 | convolution fusion | flops 279445504 | bytes 10608640 | tf_op jit(solution)/shard_map/while/body/eval_jaxpr/cond/branch_1_fun/htu,ud->thd/dot_general | solution.py:37
  115.7 2.1 fusion.4
  120.4 6.3 %conditional.4 = ((f32[4,1024]{1,0:T(4,128)S(1)}, f32[4,1024]{1,0:T(4,128)S(1)}, f32[1024,4,64]{0,2,1:T(8,128)S(1)})) conditional(s32[]{:T(128)} %clamp.12, (f32[4,1024]{1,0:T(4,128)S(1)}, f32[4,1024]{1,0:T(4,128)S(1)}, f32[1024,4,64]{0,2,1:T(8,128)S(1)}) %tuple.72, (bf16[512,64]{0,1:T(8,128)(2,1)S(1)}, ...), branch_computations={%region_4.4_spmd, %region_5.7_spmd, %region_8.10_spmd} | conditional | flops 577779200 | bytes 30369832 | solution.py:145
  122.0 2.6 %fusion.11 = f32[1024,4,64]{0,2,1:T(8,128)S(1)} fusion(f32[512,1024,4]{1,0,2:T(8,128)S(1)} %get-tuple-element.449, f32[4,1024]{1,0:T(4,128)S(1)} %get-tuple-element.538, f32[4,512]{1,0:T(4,128)S(1)} %get-tuple-element.292, f32[4,1024]{1,0:T(4,128)S(1)} %get-tuple-element.291, f32[1024,4,64]{0,2,1:T(8,128)S(1)} %get-tuple-element.294, ...), kind=kOutput, calls=%fused_computation.9 | convolution fusion | flops 279445504 | bytes 10608640 | tf_op jit(solution)/shard_map/while/body/eval_jaxpr/cond/branch_1_fun/htu,ud->thd/dot_general | solution.py:37
  124.7 2.1 fusion.4
  129.4 6.3 %conditional.4 = ((f32[4,1024]{1,0:T(4,128)S(1)}, f32[4,1024]{1,0:T(4,128)S(1)}, f32[1024,4,64]{0,2,1:T(8,128)S(1)})) conditional(s32[]{:T(128)} %clamp.12, (f32[4,1024]{1,0:T(4,128)S(1)}, f32[4,1024]{1,0:T(4,128)S(1)}, f32[1024,4,64]{0,2,1:T(8,128)S(1)}) %tuple.72, (bf16[512,64]{0,1:T(8,128)(2,1)S(1)}, ...), branch_computations={%region_4.4_spmd, %region_5.7_spmd, %region_8.10_spmd} | conditional | flops 577779200 | bytes 30369832 | solution.py:145
  131.0 2.6 %fusion.11 = f32[1024,4,64]{0,2,1:T(8,128)S(1)} fusion(f32[512,1024,4]{1,0,2:T(8,128)S(1)} %get-tuple-element.449, f32[4,1024]{1,0:T(4,128)S(1)} %get-tuple-element.538, f32[4,512]{1,0:T(4,128)S(1)} %get-tuple-element.292, f32[4,1024]{1,0:T(4,128)S(1)} %get-tuple-element.291, f32[1024,4,64]{0,2,1:T(8,128)S(1)} %get-tuple-element.294, ...), kind=kOutput, calls=%fused_computation.9 | convolution fusion | flops 279445504 | bytes 10608640 | tf_op jit(solution)/shard_map/while/body/eval_jaxpr/cond/branch_1_fun/htu,ud->thd/dot_general | solution.py:37
  133.6 2.1 fusion.4
  138.4 6.3 %conditional.4 = ((f32[4,1024]{1,0:T(4,128)S(1)}, f32[4,1024]{1,0:T(4,128)S(1)}, f32[1024,4,64]{0,2,1:T(8,128)S(1)})) conditional(s32[]{:T(128)} %clamp.12, (f32[4,1024]{1,0:T(4,128)S(1)}, f32[4,1024]{1,0:T(4,128)S(1)}, f32[1024,4,64]{0,2,1:T(8,128)S(1)}) %tuple.72, (bf16[512,64]{0,1:T(8,128)(2,1)S(1)}, ...), branch_computations={%region_4.4_spmd, %region_5.7_spmd, %region_8.10_spmd} | conditional | flops 577779200 | bytes 30369832 | solution.py:145
  140.0 2.6 %fusion.11 = f32[1024,4,64]{0,2,1:T(8,128)S(1)} fusion(f32[512,1024,4]{1,0,2:T(8,128)S(1)} %get-tuple-element.449, f32[4,1024]{1,0:T(4,128)S(1)} %get-tuple-element.538, f32[4,512]{1,0:T(4,128)S(1)} %get-tuple-element.292, f32[4,1024]{1,0:T(4,128)S(1)} %get-tuple-element.291, f32[1024,4,64]{0,2,1:T(8,128)S(1)} %get-tuple-element.294, ...), kind=kOutput, calls=%fused_computation.9 | convolution fusion | flops 279445504 | bytes 10608640 | tf_op jit(solution)/shard_map/while/body/eval_jaxpr/cond/branch_1_fun/htu,ud->thd/dot_general | solution.py:37
  147.4 6.3 %conditional.4 = ((f32[4,1024]{1,0:T(4,128)S(1)}, f32[4,1024]{1,0:T(4,128)S(1)}, f32[1024,4,64]{0,2,1:T(8,128)S(1)})) conditional(s32[]{:T(128)} %clamp.12, (f32[4,1024]{1,0:T(4,128)S(1)}, f32[4,1024]{1,0:T(4,128)S(1)}, f32[1024,4,64]{0,2,1:T(8,128)S(1)}) %tuple.72, (bf16[512,64]{0,1:T(8,128)(2,1)S(1)}, ...), branch_computations={%region_4.4_spmd, %region_5.7_spmd, %region_8.10_spmd} | conditional | flops 577779200 | bytes 30369832 | solution.py:145
  149.0 2.6 %fusion.11 = f32[1024,4,64]{0,2,1:T(8,128)S(1)} fusion(f32[512,1024,4]{1,0,2:T(8,128)S(1)} %get-tuple-element.449, f32[4,1024]{1,0:T(4,128)S(1)} %get-tuple-element.538, f32[4,512]{1,0:T(4,128)S(1)} %get-tuple-element.292, f32[4,1024]{1,0:T(4,128)S(1)} %get-tuple-element.291, f32[1024,4,64]{0,2,1:T(8,128)S(1)} %get-tuple-element.294, ...), kind=kOutput, calls=%fused_computation.9 | convolution fusion | flops 279445504 | bytes 10608640 | tf_op jit(solution)/shard_map/while/body/eval_jaxpr/cond/branch_1_fun/htu,ud->thd/dot_general | solution.py:37
  156.3 6.3 %conditional.4 = ((f32[4,1024]{1,0:T(4,128)S(1)}, f32[4,1024]{1,0:T(4,128)S(1)}, f32[1024,4,64]{0,2,1:T(8,128)S(1)})) conditional(s32[]{:T(128)} %clamp.12, (f32[4,1024]{1,0:T(4,128)S(1)}, f32[4,1024]{1,0:T(4,128)S(1)}, f32[1024,4,64]{0,2,1:T(8,128)S(1)}) %tuple.72, (bf16[512,64]{0,1:T(8,128)(2,1)S(1)}, ...), branch_computations={%region_4.4_spmd, %region_5.7_spmd, %region_8.10_spmd} | conditional | flops 577779200 | bytes 30369832 | solution.py:145
  157.9 2.6 %fusion.11 = f32[1024,4,64]{0,2,1:T(8,128)S(1)} fusion(f32[512,1024,4]{1,0,2:T(8,128)S(1)} %get-tuple-element.449, f32[4,1024]{1,0:T(4,128)S(1)} %get-tuple-element.538, f32[4,512]{1,0:T(4,128)S(1)} %get-tuple-element.292, f32[4,1024]{1,0:T(4,128)S(1)} %get-tuple-element.291, f32[1024,4,64]{0,2,1:T(8,128)S(1)} %get-tuple-element.294, ...), kind=kOutput, calls=%fused_computation.9 | convolution fusion | flops 279445504 | bytes 10608640 | tf_op jit(solution)/shard_map/while/body/eval_jaxpr/cond/branch_1_fun/htu,ud->thd/dot_general | solution.py:37
  165.3 6.3 %conditional.4 = ((f32[4,1024]{1,0:T(4,128)S(1)}, f32[4,1024]{1,0:T(4,128)S(1)}, f32[1024,4,64]{0,2,1:T(8,128)S(1)})) conditional(s32[]{:T(128)} %clamp.12, (f32[4,1024]{1,0:T(4,128)S(1)}, f32[4,1024]{1,0:T(4,128)S(1)}, f32[1024,4,64]{0,2,1:T(8,128)S(1)}) %tuple.72, (bf16[512,64]{0,1:T(8,128)(2,1)S(1)}, ...), branch_computations={%region_4.4_spmd, %region_5.7_spmd, %region_8.10_spmd} | conditional | flops 577779200 | bytes 30369832 | solution.py:145
  166.9 2.6 %fusion.11 = f32[1024,4,64]{0,2,1:T(8,128)S(1)} fusion(f32[512,1024,4]{1,0,2:T(8,128)S(1)} %get-tuple-element.449, f32[4,1024]{1,0:T(4,128)S(1)} %get-tuple-element.538, f32[4,512]{1,0:T(4,128)S(1)} %get-tuple-element.292, f32[4,1024]{1,0:T(4,128)S(1)} %get-tuple-element.291, f32[1024,4,64]{0,2,1:T(8,128)S(1)} %get-tuple-element.294, ...), kind=kOutput, calls=%fused_computation.9 | convolution fusion | flops 279445504 | bytes 10608640 | tf_op jit(solution)/shard_map/while/body/eval_jaxpr/cond/branch_1_fun/htu,ud->thd/dot_general | solution.py:37
  174.3 6.3 %conditional.4 = ((f32[4,1024]{1,0:T(4,128)S(1)}, f32[4,1024]{1,0:T(4,128)S(1)}, f32[1024,4,64]{0,2,1:T(8,128)S(1)})) conditional(s32[]{:T(128)} %clamp.12, (f32[4,1024]{1,0:T(4,128)S(1)}, f32[4,1024]{1,0:T(4,128)S(1)}, f32[1024,4,64]{0,2,1:T(8,128)S(1)}) %tuple.72, (bf16[512,64]{0,1:T(8,128)(2,1)S(1)}, ...), branch_computations={%region_4.4_spmd, %region_5.7_spmd, %region_8.10_spmd} | conditional | flops 577779200 | bytes 30369832 | solution.py:145
  175.9 2.6 %fusion.11 = f32[1024,4,64]{0,2,1:T(8,128)S(1)} fusion(f32[512,1024,4]{1,0,2:T(8,128)S(1)} %get-tuple-element.449, f32[4,1024]{1,0:T(4,128)S(1)} %get-tuple-element.538, f32[4,512]{1,0:T(4,128)S(1)} %get-tuple-element.292, f32[4,1024]{1,0:T(4,128)S(1)} %get-tuple-element.291, f32[1024,4,64]{0,2,1:T(8,128)S(1)} %get-tuple-element.294, ...), kind=kOutput, calls=%fused_computation.9 | convolution fusion | flops 279445504 | bytes 10608640 | tf_op jit(solution)/shard_map/while/body/eval_jaxpr/cond/branch_1_fun/htu,ud->thd/dot_general | solution.py:37
  183.3 6.3 %conditional.4 = ((f32[4,1024]{1,0:T(4,128)S(1)}, f32[4,1024]{1,0:T(4,128)S(1)}, f32[1024,4,64]{0,2,1:T(8,128)S(1)})) conditional(s32[]{:T(128)} %clamp.12, (f32[4,1024]{1,0:T(4,128)S(1)}, f32[4,1024]{1,0:T(4,128)S(1)}, f32[1024,4,64]{0,2,1:T(8,128)S(1)}) %tuple.72, (bf16[512,64]{0,1:T(8,128)(2,1)S(1)}, ...), branch_computations={%region_4.4_spmd, %region_5.7_spmd, %region_8.10_spmd} | conditional | flops 577779200 | bytes 30369832 | solution.py:145
  184.9 2.6 %fusion.11 = f32[1024,4,64]{0,2,1:T(8,128)S(1)} fusion(f32[512,1024,4]{1,0,2:T(8,128)S(1)} %get-tuple-element.449, f32[4,1024]{1,0:T(4,128)S(1)} %get-tuple-element.538, f32[4,512]{1,0:T(4,128)S(1)} %get-tuple-element.292, f32[4,1024]{1,0:T(4,128)S(1)} %get-tuple-element.291, f32[1024,4,64]{0,2,1:T(8,128)S(1)} %get-tuple-element.294, ...), kind=kOutput, calls=%fused_computation.9 | convolution fusion | flops 279445504 | bytes 10608640 | tf_op jit(solution)/shard_map/while/body/eval_jaxpr/cond/branch_1_fun/htu,ud->thd/dot_general | solution.py:37
  192.3 6.3 %conditional.4 = ((f32[4,1024]{1,0:T(4,128)S(1)}, f32[4,1024]{1,0:T(4,128)S(1)}, f32[1024,4,64]{0,2,1:T(8,128)S(1)})) conditional(s32[]{:T(128)} %clamp.12, (f32[4,1024]{1,0:T(4,128)S(1)}, f32[4,1024]{1,0:T(4,128)S(1)}, f32[1024,4,64]{0,2,1:T(8,128)S(1)}) %tuple.72, (bf16[512,64]{0,1:T(8,128)(2,1)S(1)}, ...), branch_computations={%region_4.4_spmd, %region_5.7_spmd, %region_8.10_spmd} | conditional | flops 577779200 | bytes 30369832 | solution.py:145
  193.9 2.6 %fusion.11 = f32[1024,4,64]{0,2,1:T(8,128)S(1)} fusion(f32[512,1024,4]{1,0,2:T(8,128)S(1)} %get-tuple-element.449, f32[4,1024]{1,0:T(4,128)S(1)} %get-tuple-element.538, f32[4,512]{1,0:T(4,128)S(1)} %get-tuple-element.292, f32[4,1024]{1,0:T(4,128)S(1)} %get-tuple-element.291, f32[1024,4,64]{0,2,1:T(8,128)S(1)} %get-tuple-element.294, ...), kind=kOutput, calls=%fused_computation.9 | convolution fusion | flops 279445504 | bytes 10608640 | tf_op jit(solution)/shard_map/while/body/eval_jaxpr/cond/branch_1_fun/htu,ud->thd/dot_general | solution.py:37
  196.5 2.1 fusion.4
  201.2 6.3 %conditional.4 = ((f32[4,1024]{1,0:T(4,128)S(1)}, f32[4,1024]{1,0:T(4,128)S(1)}, f32[1024,4,64]{0,2,1:T(8,128)S(1)})) conditional(s32[]{:T(128)} %clamp.12, (f32[4,1024]{1,0:T(4,128)S(1)}, f32[4,1024]{1,0:T(4,128)S(1)}, f32[1024,4,64]{0,2,1:T(8,128)S(1)}) %tuple.72, (bf16[512,64]{0,1:T(8,128)(2,1)S(1)}, ...), branch_computations={%region_4.4_spmd, %region_5.7_spmd, %region_8.10_spmd} | conditional | flops 577779200 | bytes 30369832 | solution.py:145
  202.8 2.6 %fusion.11 = f32[1024,4,64]{0,2,1:T(8,128)S(1)} fusion(f32[512,1024,4]{1,0,2:T(8,128)S(1)} %get-tuple-element.449, f32[4,1024]{1,0:T(4,128)S(1)} %get-tuple-element.538, f32[4,512]{1,0:T(4,128)S(1)} %get-tuple-element.292, f32[4,1024]{1,0:T(4,128)S(1)} %get-tuple-element.291, f32[1024,4,64]{0,2,1:T(8,128)S(1)} %get-tuple-element.294, ...), kind=kOutput, calls=%fused_computation.9 | convolution fusion | flops 279445504 | bytes 10608640 | tf_op jit(solution)/shard_map/while/body/eval_jaxpr/cond/branch_1_fun/htu,ud->thd/dot_general | solution.py:37
  210.2 9.1 %conditional.4 = ((f32[4,1024]{1,0:T(4,128)S(1)}, f32[4,1024]{1,0:T(4,128)S(1)}, f32[1024,4,64]{0,2,1:T(8,128)S(1)})) conditional(s32[]{:T(128)} %clamp.12, (f32[4,1024]{1,0:T(4,128)S(1)}, f32[4,1024]{1,0:T(4,128)S(1)}, f32[1024,4,64]{0,2,1:T(8,128)S(1)}) %tuple.72, (bf16[512,64]{0,1:T(8,128)(2,1)S(1)}, ...), branch_computations={%region_4.4_spmd, %region_5.7_spmd, %region_8.10_spmd} | conditional | flops 577779200 | bytes 30369832 | solution.py:145
  210.6 2.4 fusion.23
  213.0 3.2 %fusion.30 = f32[1024,4,64]{0,2,1:T(8,128)S(1)} fusion(f32[512,1024,4]{1,0,2:T(8,128)S(1)} %get-tuple-element.451, f32[4,1024]{1,0:T(4,128)S(1)} %get-tuple-element.541, f32[4,512]{1,0:T(4,128)S(1)} %get-tuple-element.303, f32[4,1024]{1,0:T(4,128)S(1)} %get-tuple-element.302, pred[1024,512]{0,1:T(8,128)(4,1)S(1)} %broadcast_compare_fusion, ...), kind=kOutput, calls=%fused_computation.27 | convolution fusion | flops 283639808 | bytes 11132928 | tf_op jit(solution)/shard_map/while/body/eval_jaxpr/cond/branch_2_fun/htu,ud->thd/dot_general | solution.py:37
  216.2 3.1 %fusion.22 = f32[4,1024]{1,0:T(4,128)S(1)} fusion(f32[512,1024,4]{1,0,2:T(8,128)S(1)} %get-tuple-element.451, f32[4,1024]{1,0:T(4,128)S(1)} %get-tuple-element.541, f32[4,512]{1,0:T(4,128)S(1)} %get-tuple-element.303, f32[4,1024]{1,0:T(4,128)S(1)} %get-tuple-element.302, pred[1024,512]{0,1:T(8,128)(4,1)S(1)} %broadcast_compare_fusion), kind=kLoop, calls=%fused_computation.22 | loop fusion | flops 14675968 | bytes 8970240 | tf_op jit(solution)/shard_map/while/body/eval_jaxpr/cond/branch_2_fun/reduce_sum | solution.py:36
  221.9 9.1 %conditional.4 = ((f32[4,1024]{1,0:T(4,128)S(1)}, f32[4,1024]{1,0:T(4,128)S(1)}, f32[1024,4,64]{0,2,1:T(8,128)S(1)})) conditional(s32[]{:T(128)} %clamp.12, (f32[4,1024]{1,0:T(4,128)S(1)}, f32[4,1024]{1,0:T(4,128)S(1)}, f32[1024,4,64]{0,2,1:T(8,128)S(1)}) %tuple.72, (bf16[512,64]{0,1:T(8,128)(2,1)S(1)}, ...), branch_computations={%region_4.4_spmd, %region_5.7_spmd, %region_8.10_spmd} | conditional | flops 577779200 | bytes 30369832 | solution.py:145
  222.3 2.4 fusion.23
  224.7 3.2 %fusion.30 = f32[1024,4,64]{0,2,1:T(8,128)S(1)} fusion(f32[512,1024,4]{1,0,2:T(8,128)S(1)} %get-tuple-element.451, f32[4,1024]{1,0:T(4,128)S(1)} %get-tuple-element.541, f32[4,512]{1,0:T(4,128)S(1)} %get-tuple-element.303, f32[4,1024]{1,0:T(4,128)S(1)} %get-tuple-element.302, pred[1024,512]{0,1:T(8,128)(4,1)S(1)} %broadcast_compare_fusion, ...), kind=kOutput, calls=%fused_computation.27 | convolution fusion | flops 283639808 | bytes 11132928 | tf_op jit(solution)/shard_map/while/body/eval_jaxpr/cond/branch_2_fun/htu,ud->thd/dot_general | solution.py:37
  227.9 3.1 %fusion.22 = f32[4,1024]{1,0:T(4,128)S(1)} fusion(f32[512,1024,4]{1,0,2:T(8,128)S(1)} %get-tuple-element.451, f32[4,1024]{1,0:T(4,128)S(1)} %get-tuple-element.541, f32[4,512]{1,0:T(4,128)S(1)} %get-tuple-element.303, f32[4,1024]{1,0:T(4,128)S(1)} %get-tuple-element.302, pred[1024,512]{0,1:T(8,128)(4,1)S(1)} %broadcast_compare_fusion), kind=kLoop, calls=%fused_computation.22 | loop fusion | flops 14675968 | bytes 8970240 | tf_op jit(solution)/shard_map/while/body/eval_jaxpr/cond/branch_2_fun/reduce_sum | solution.py:36
  231.6 11.5 %all_to_all.35 = bf16[4,256,256]{1,2,0:T(8,128)(2,1)S(1)} all-to-all(bf16[4,256,256]{1,2,0:T(8,128)(2,1)S(1)} %copy.41), channel_id=1, replica_groups=mesh['sp'=8,'tp'=4] {'tp'}, dimensions={0} | all-to-all | bytes 1048576 | tf_op jit(solution)/shard_map/all_to_all | solution.py:153
  243.1 4.4 %convolution_convert_fusion = bf16[256,2048]{1,0:T(8,128)(2,1)} fusion(bf16[256,1024]{0,1:T(8,128)(2,1)S(1)} %bitcast.110, bf16[1024,2048]{1,0:T(8,128)(2,1)} %param.22), kind=kOutput, calls=%fused_computation.44 | convolution fusion | flops 1074266112 | bytes 5767168 | tf_op jit(solution)/shard_map/dot_general | solution.py:154
  (228 shorter events, 81.9 us)
Async XLA Ops:
  6.5 1.6 copy-start
  6.5 75.2 %all-gather.2.cloned.1.call-start = ((), (), s32[]{:S(2)}) async-start(), calls=%async_computation.2 | async-start | bytes 2359296 | tf_op jit(solution)/shard_map/all_gather | solution.py:105
  8.1 10.6 %copy-start.3 = (f32[64]{0:T(128)S(1)}, f32[64]{0:T(128)}, u32[]{:S(2)}) copy-start(f32[64]{0:T(128)} %param.19) | copy-start | bytes 772
  8.1 10.7 %copy-start.2 = (f32[64]{0:T(128)S(1)}, f32[64]{0:T(128)}, u32[]{:S(2)}) copy-start(f32[64]{0:T(128)} %param.20) | copy-start | bytes 772
  16.7 17.9 %copy-start.1 = (f32[1024,4]{0,1:T(4,128)S(1)}, f32[1024,4]{0,1:T(4,128)}, u32[]{:S(2)}) copy-start(f32[1024,4]{0,1:T(4,128)} %param.21) | copy-start | bytes 49156
Sparse Core Ops, SparseCore 0:
  34.7 46.9 all-gather.1
where the time goes:
time: 255 us; the launch traced here: 254 us
  matrix products  82.4 us (32%)
  blocking collectives  56.9 us (22%)
  other arithmetic  38.4 us (15%)
  local copies, waits for them, and re-layouts  34.4 us (13%)
  waiting for transfers between devices  15.7 us (6%)
  between operations  13.6 us (5%)
  loops' own time  13 us (5%)
    dot_general x16, matrix products, attend_step(): jnp.einsum('htu,ud->thd', weights_exp.astype(jnp.bfloat16), value_slice,...  42.9 us
    reduce_sum x16, other arithmetic, attend_step(): total_new = total * rescale + jnp.sum(weights_exp, axis=-1)  35 us
    all_gather x1, blocking collectives, per_device(): all_decays = lax.all_gather(decay_sums, 'sp', axis=0, tiled=True)  31.2 us
    dot_general x16, matrix products, attend_step(): jnp.einsum('thd,ud->htu', query_rows, key_slice, preferred_element_type=j...  26.4 us
    slice x16, local copies, waits for them, and re-layouts, one_block(): value_slice = pair_slice[:, head_size:]  17.6 us
    all_gather x1, waiting for transfers between devices, per_device(): pieces = lax.all_gather(key_values, 'sp', axis=0, tiled=True)  15.7 us
    all_to_all x1, blocking collectives, per_device(): lax.all_to_all(packed, 'tp', split_axis=1, concat_axis=0, tiled=True)[:, 0]  14.2 us
    another operation x1, loops' own time, per_device(): lax.scan(one_block, state, jnp.arange(piece_rows // key_block, dtype=jnp....  11.8 us
  transfers between devices with their start and end apart: 1, of which 1 were waited for; matrix products, arithmetic and copies ran while one was open for 0% of the time, Pallas kernels for 0%

commit v1 on v0

v1 whole, which is shorter than its diff:
```python
import math

import jax
import jax.numpy as jnp
from jax import lax
from jax.experimental import pallas as pl
from jax.experimental.pallas import tpu as pltpu
from jax.sharding import Mesh, PartitionSpec as P

epsilon = 1e-06
LOG2E = math.log2(math.e)
ALL = ("sp", "kv", "half")
HEADS_PER_DOT = 2


def rms_norm(vector, gain_vec):
    return (
        vector * lax.rsqrt(jnp.mean(vector * vector, axis=-1, keepdims=True) + epsilon) * gain_vec
    )


def attend_kernel(
    place_ref, queries_ref, decay_ref, packed_ref, out_ref, kv_ref, ones_ref, q_ref, peak_ref,
    acc_ref, sems, *, rows, heads, half_count, tp_count, key_block
):
    members = packed_ref.shape[0]
    blocks = 2 * members
    group = place_ref[2]
    copies = []
    for j in range(members):
        block = (j // half_count) * tp_count + group * half_count + j % half_count
        for part, where in ((0, block), (1, blocks - 1 - block)):
            copies.append(
                pltpu.make_async_copy(
                    packed_ref.at[j, pl.ds(part * rows, rows)],
                    kv_ref.at[pl.ds(pl.multiple_of(where * rows, rows), rows)],
                    sems.at[2 * j + part],
                )
            )
            copies[-1].start()
    lane = lax.broadcasted_iota(jnp.int32, (rows, 128), 1)
    low = lane < 64
    for r in range(2):
        for pair in range(heads // 2):
            both = queries_ref[r, :, pair * 128 : (pair + 1) * 128].astype(jnp.float32)
            even = jnp.where(low, both, 0.0)
            odd = jnp.where(low, pltpu.roll(both, 64, 1), 0.0)
            q_ref[r, (2 * pair) * rows : (2 * pair + 1) * rows] = even.astype(jnp.bfloat16)
            q_ref[r, (2 * pair + 1) * rows : (2 * pair + 2) * rows] = odd.astype(jnp.bfloat16)
    for copy in copies:
        copy.wait()

    def fill(i, carry):
        at = pl.ds(pl.multiple_of(i * key_block, key_block), key_block)
        wide = lax.broadcasted_iota(jnp.int32, (key_block, 128), 1) < 64
        ones_ref[at] = jnp.where(wide, 1.0, kv_ref[at].astype(jnp.float32)).astype(jnp.bfloat16)
        return carry

    lax.fori_loop(0, kv_ref.shape[0] // key_block, fill, 0)
    span = HEADS_PER_DOT * rows

    for r in range(2):
        first = place_ref[r]
        peak_ref[...] = jnp.full_like(peak_ref, -1e30)
        acc_ref[...] = jnp.zeros_like(acc_ref)

        def step(index, masked):
            at = pl.ds(pl.multiple_of(index * key_block, key_block), key_block)
            keys = kv_ref[at]
            values = ones_ref[at]
            for start in range(0, heads, HEADS_PER_DOT):
                part = pl.ds(start * rows, span)
                scores = lax.dot_general(
                    q_ref[r, part], keys, (((1,), (1,)), ((), ())),
                    preferred_element_type=jnp.float32,
                )
                scores = scores.reshape(HEADS_PER_DOT, rows, key_block)
                scores = scores - decay_ref[index, start : start + HEADS_PER_DOT][:, None, :]
                if masked:
                    row = first + lax.broadcasted_iota(jnp.int32, (rows, key_block), 0)
                    col = index * key_block + lax.broadcasted_iota(
                        jnp.int32, (rows, key_block), 1
                    )
                    scores = jnp.where((col <= row)[None], scores, -1e30)
                scores = scores.reshape(span, key_block)
                before = peak_ref[part]
                after = jnp.maximum(before, jnp.max(scores, axis=1, keepdims=True))
                weights = jnp.exp2(scores - after[:, :1]).astype(jnp.bfloat16)
                acc_ref[part] = acc_ref[part] * jnp.exp2(before - after) + jnp.dot(
                    weights, values, preferred_element_type=jnp.float32
                )
                peak_ref[part] = after

        full = first // key_block

        def body(index, carry):
            step(index, False)
            return carry

        lax.fori_loop(0, full, body, 0)
        step(full, True)
        for pair in range(heads // 2):
            even = acc_ref[(2 * pair) * rows : (2 * pair + 1) * rows]
            odd = acc_ref[(2 * pair + 1) * rows : (2 * pair + 2) * rows]
            done = jnp.where(low, pltpu.roll(even, 64, 1), odd) / jnp.where(
                low, even, pltpu.roll(odd, 64, 1)
            )
            out_ref[r, :, pair * 128 : (pair + 1) * 128] = done.astype(jnp.bfloat16)


def per_device(inputs, in_gain, w_query, w_key, w_value, query_gain, key_gain, decay_sums, w_out):
    sp_count = lax.axis_size("sp")
    kv_heads = lax.axis_size("kv")
    half_count = lax.axis_size("half")
    tp_count = kv_heads * half_count
    group = lax.axis_index("kv")
    me = (lax.axis_index("sp") * kv_heads + group) * half_count + lax.axis_index("half")
    count = sp_count * tp_count
    mirror = [(i, count - 1 - i) for i in range(count)]
    head_size = query_gain.shape[0]
    rows = inputs.shape[0]
    length = rows * count
    all_heads = w_query.shape[1] // head_size
    heads = all_heads // kv_heads
    width = heads * head_size
    members = sp_count * half_count
    key_block = math.gcd(length, 512)

    def choose(a, b):
        return jnp.where(group == 0, a, b)

    normed = rms_norm(inputs.astype(jnp.float32), in_gain).astype(jnp.bfloat16)
    keys = rms_norm(
        jnp.dot(normed, w_key, preferred_element_type=jnp.float32).reshape(
            rows, kv_heads, head_size
        ),
        key_gain,
    ).astype(jnp.bfloat16)
    values = (
        jnp.dot(normed, w_value, preferred_element_type=jnp.float32)
        .astype(jnp.bfloat16)
        .reshape(rows, kv_heads, head_size)
    )
    pairs = jnp.concatenate([keys, values], axis=2)
    own_kv = choose(pairs[:, 0], pairs[:, 1])
    far_kv = lax.ppermute(choose(pairs[:, 1], pairs[:, 0]), ALL, mirror)

    decays = decay_sums.T * LOG2E
    high = lax.reduce_precision(decays, 8, 7)
    rest = decays - high
    middle = lax.reduce_precision(rest, 8, 7)
    pieces = jnp.stack([high, middle, rest - middle]).astype(jnp.bfloat16)
    packed = jnp.concatenate([own_kv, far_kv, pieces.reshape(-1, 128)], axis=0)
    gathered = lax.all_gather(packed, ("sp", "half"), axis=0, tiled=False)

    queries = rms_norm(
        jnp.dot(normed, w_query, preferred_element_type=jnp.float32).reshape(
            rows, all_heads, head_size
        ),
        query_gain * (LOG2E * head_size ** (-0.5)),
    ).astype(jnp.bfloat16).reshape(rows, kv_heads * width)
    own_q = choose(queries[:, :width], queries[:, width:])
    far_q = lax.ppermute(choose(queries[:, width:], queries[:, :width]), ALL, mirror)

    decay_all = jnp.sum(
        gathered[:, 2 * rows :].reshape(sp_count, half_count, 3, -1, 128).astype(jnp.float32),
        axis=2,
    ).reshape(sp_count, heads, -1, key_block)
    decay_all = decay_all.transpose(0, 2, 1, 3).reshape(length // key_block, heads, key_block)
    place = jnp.stack([me * rows, (count - 1 - me) * rows, group]).astype(jnp.int32)
    vmem = pl.BlockSpec(memory_space=pltpu.VMEM)
    attended = pl.pallas_call(
        lambda *refs: attend_kernel(
            *refs, rows=rows, heads=heads, half_count=half_count, tp_count=tp_count,
            key_block=key_block,
        ),
        out_shape=jax.ShapeDtypeStruct((2, rows, width), jnp.bfloat16),
        in_specs=[
            pl.BlockSpec(memory_space=pltpu.SMEM), vmem, vmem, pl.BlockSpec(memory_space=pl.ANY)
        ],
        out_specs=vmem,
        scratch_shapes=[
            pltpu.VMEM((length, 128), jnp.bfloat16),
            pltpu.VMEM((length, 128), jnp.bfloat16),
            pltpu.VMEM((2, heads * rows, 128), jnp.bfloat16),
            pltpu.VMEM((heads * rows, 128), jnp.float32),
            pltpu.VMEM((heads * rows, 128), jnp.float32),
            pltpu.SemaphoreType.DMA((2 * members,)),
        ],
        compiler_params=pltpu.CompilerParams(vmem_limit_bytes=48 * 1024 * 1024),
        name="attend",
    )(place, jnp.stack([own_q, far_q]), decay_all, gathered)
    back = lax.ppermute(attended[1], ALL, mirror)
    whole = choose(
        jnp.concatenate([attended[0], back], axis=1), jnp.concatenate([back, attended[0]], axis=1)
    )
    return jnp.dot(whole, w_out, preferred_element_type=jnp.float32).astype(jnp.bfloat16)


def solution(mesh):
    sp_count, tp_count = mesh.devices.shape
    split = Mesh(mesh.devices.reshape(sp_count, 2, tp_count // 2), ALL)
    placed = (P(ALL, None), P(), P(), P(), P(), P(), P(), P("sp", ("kv", "half")), P())
    return jax.shard_map(
        per_device, mesh=split, in_specs=placed, out_specs=P(ALL, None), check_vma=False
    )
```

time: 255 us -> 151 us (0.59)
  the two profiles are of different devices: /device:TPU:28 before, /device:TPU:9 now
where the time goes in v1:
time: 151 us; the launch traced here: 150 us
  waiting for transfers between devices  58.6 us (39%)
  Pallas kernels  50.7 us (34%)
  between operations  13.6 us (9%)
  matrix products  9.27 us (6%)
  starting transfers between devices  7.89 us (5%)
  local copies, waits for them, and re-layouts  5.22 us (3%)
  other arithmetic  5.12 us (3%)
    pallas_call x1, Pallas kernels, per_device(): pl.pallas_call(lambda *refs: attend_kernel(*refs, rows=rows, heads=heads,...  50.7 us
    all_gather x1, waiting for transfers between devices, per_device(): gathered = lax.all_gather(packed, ('sp', 'half'), axis=0, tiled=False)  22.7 us
    ppermute x1, waiting for transfers between devices, per_device(): lax.ppermute(choose(queries[:, width:], queries[:, :width]), ALL, mirror)  18.2 us
    ppermute x1, waiting for transfers between devices, per_device(): back = lax.ppermute(attended[1], ALL, mirror)  13.9 us
    dot_general x1, matrix products, per_device(): jnp.dot(normed, w_query, preferred_element_type=jnp.float32)  4.48 us
    ppermute x1, waiting for transfers between devices, per_device(): far_kv = lax.ppermute(choose(pairs[:, 1], pairs[:, 0]), ALL, mirror)  3.84 us
    ppermute x1, starting transfers between devices, per_device(): far_kv = lax.ppermute(choose(pairs[:, 1], pairs[:, 0]), ALL, mirror)  3.81 us
  transfers between devices with their start and end apart: 4, of which 4 were waited for; matrix products, arithmetic and copies ran while one was open for 5% of the time, Pallas kernels for 0%

profile of v1, /device:TPU:9, one launch (start us, length us, event | category | flops | bytes accessed | tf_op | source)
XLA Modules:
  0.0 150.4 jit_solution(5658468627250099318)
XLA Ops:
  6.5 0.0 copy-start
  6.5 0.0 copy-start.2
  6.5 0.0 copy-start.6
  6.5 0.0 all-gather.3.cloned.1.call-start
  6.6 1.6 %fusion = f32[256]{0:T(256)S(1)} fusion(bf16[256,2048]{1,0:T(8,128)(2,1)} %param.9), kind=kLoop, calls=%fused_computation.3 | loop fusion | flops 1572608 | bytes 1049600 | tf_op jit(solution)/shard_map/reduce_sum | solution.py:18
  8.2 0.0 copy-start.4
  8.2 2.0 %convolution_convert_fusion.1 = bf16[256,128]{0,1:T(8,128)(2,1)S(1)} fusion(bf16[2048,128]{1,0:T(8,128)(2,1)} %param.13, bf16[256,2048]{1,0:T(8,128)(2,1)} %param.9, f32[2048]{0:T(1024)} %param.10, f32[256]{0:T(256)S(1)} %add_rsqrt_fusion.2), kind=kOutput, calls=%fused_computation.6 | convolution fusion | flops 136347648 | bytes 1647616 | tf_op jit(solution)/shard_map/dot_general | solution.py:140
  10.2 0.0 copy-start.3
  10.2 0.1 copy.15
  10.3 0.0 copy-done
  10.3 0.0 copy-done.2
  10.3 0.0 copy-done.6
  10.3 0.6 multiply_reduce_fusion
  10.9 0.1 copy.14
  11.1 0.0 copy-done.4
  11.1 0.1 multiply_convert_fusion.1
  11.2 0.1 select_bitcast_fusion.2
  11.3 0.1 select_bitcast_fusion.1
  11.4 3.8 %collective-permute-start.1 = (bf16[256,128]{1,0:T(8,128)(2,1)S(1)}, bf16[256,128]{1,0:T(8,128)(2,1)S(1)}, u32[]{:S(2)}, u32[]{:S(2)}) collective-permute-start(bf16[256,128]{1,0:T(8,128)(2,1)S(1)} %select_bitcast_fusion.1), channel_id=1, source_target_pairs={{0,31},{1,30},{2,29},{3,28},{4,27},{5,26},{6,25},{7,24},{8,23},{9,... | collective-permute-start | bytes 196616 | tf_op jit(solution)/shard_map/ppermute | solution.py:146
  15.2 0.0 copy-done.3
  15.3 3.8 %collective-permute-done.1 = bf16[256,128]{1,0:T(8,128)(2,1)S(1)} collective-permute-done((bf16[256,128]{1,0:T(8,128)(2,1)S(1)}, bf16[256,128]{1,0:T(8,128)(2,1)S(1)}, u32[]{:S(2)}, u32[]{:S(2)}) %collective-permute-start.1) | collective-permute-done | bytes 65568 | tf_op jit(solution)/shard_map/ppermute | solution.py:146
  19.2 0.7 pad_maximum_fusion.1
  19.8 0.0 all-gather.3.cloned.1.call-update
  19.8 4.5 %fusion.20 = (f32[256,1024]{1,0:T(8,128)S(1)}, f32[256,1024]{1,0:T(8,128)}) fusion(bf16[2048,1024]{1,0:T(8,128)(2,1)} %param.11, bf16[256,2048]{1,0:T(8,128)(2,1)S(1)} %copy-done.2, f32[2048]{0:T(1024)S(1)} %copy-done.6, f32[256]{0:T(256)S(1)} %add_rsqrt_fusion.2), kind=kOutput, calls=%fused_computation.48 | convolution fusion | flops 1076101120 | bytes 7349248 | tf_op jit(solution)/shard_map/dot_general | solution.py:157
  24.3 0.3 copy.12
  24.7 0.0 copy-start.7
  24.7 0.1 bitcast_reduce_fusion
  24.8 0.1 mul.106
  24.9 0.3 copy.13
  25.2 0.1 copy-done.7
  25.3 0.1 mul.112
  25.4 1.4 multiply_convert_fusion
  26.9 2.3 %collective-permute-start = (bf16[256,512]{1,0:T(8,128)(2,1)S(1)}, bf16[256,512]{1,0:T(8,128)(2,1)S(1)}, u32[]{:S(2)}, u32[]{:S(2)}) collective-permute-start(bf16[256,512]{1,0:T(8,128)(2,1)S(1)} %get-tuple-element.10), channel_id=1, source_target_pairs={{0,31},{1,30},{2,29},{3,28},{4,27},{5,26},{6,25},{7,24},{8,23},{9,... | collective-permute-start | bytes 786440 | tf_op jit(solution)/shard_map/ppermute | solution.py:163
  29.2 0.1 pad_add_fusion.refs_0_
  29.3 18.2 %collective-permute-done = bf16[256,512]{1,0:T(8,128)(2,1)S(1)} collective-permute-done((bf16[256,512]{1,0:T(8,128)(2,1)S(1)}, bf16[256,512]{1,0:T(8,128)(2,1)S(1)}, u32[]{:S(2)}, u32[]{:S(2)}) %collective-permute-start) | collective-permute-done | bytes 262176 | tf_op jit(solution)/shard_map/ppermute | solution.py:163
  47.5 0.1 pad_maximum_fusion.refs_1_
  47.5 22.7 %all-gather.3.cloned.1.call-done = bf16[9728,128]{1,0:T(8,128)(2,1)} async-done(((bf16[608,128]{1,0:T(8,128)(2,1)}), bf16[9728,128]{1,0:T(8,128)(2,1)}) %all-gather.3.cloned.1.call-update) | async-done | bytes 2490384 | tf_op jit(solution)/shard_map/all_gather | solution.py:154
  70.2 1.2 slice.37
  71.4 0.8 convert_reduce_fusion
  72.1 1.8 %reshape.56 = f32[8,8,2,512]{3,2,1,0:T(2,128)} reshape(f32[8,2,32,128]{3,2,1,0:T(8,128)} %convert_reduce_fusion) | data formatting | bytes 524288 | tf_op jit(solution)/shard_map/reshape | solution.py:168
  73.9 1.0 copy.16
  74.9 0.0 copy-done.1
  74.9 0.0 copy-start.5
  74.9 50.7 %attend.1 = bf16[2,256,512]{2,1,0:T(8,128)(2,1)S(1)} custom-call(s32[3]{0:T(128)S(1)} %pad_add_fusion.refs_0_, bf16[2,256,512]{2,1,0:T(8,128)(2,1)S(1)} %pad_maximum_fusion.refs_1_, f32[16,8,512]{2,1,0:T(8,128)S(1)} %bitcast.52, bf16[16,608,128]{2,1,0:T(8,128)(2,1)S(1)} %bitcast.51), custom_call_target="tpu_custom_call" | custom-call | tf_op jit(solution)/shard_map/attend/pallas_call | solution.py:172
  125.6 1.8 %collective-permute-start.2 = (bf16[256,512]{1,0:T(8,128)(2,1)S(1)}, bf16[256,512]{1,0:T(8,128)(2,1)S(1)}, u32[]{:S(2)}, u32[]{:S(2)}) collective-permute-start(bf16[256,512]{1,0:T(8,128)(2,1)S(1)} %get-tuple-element.8), channel_id=1, source_target_pairs={{0,31},{1,30},{2,29},{3,28},{4,27},{5,26},{6,25},{7,24},{8,23},{9,... | collective-permute-start | bytes 786440 | tf_op jit(solution)/shard_map/ppermute | solution.py:193
  127.4 13.9 %collective-permute-done.2 = bf16[256,512]{1,0:T(8,128)(2,1)S(1)} collective-permute-done((bf16[256,512]{1,0:T(8,128)(2,1)S(1)}, bf16[256,512]{1,0:T(8,128)(2,1)S(1)}, u32[]{:S(2)}, u32[]{:S(2)}) %collective-permute-start.2) | collective-permute-done | bytes 262176 | tf_op jit(solution)/shard_map/ppermute | solution.py:193
  141.3 0.0 copy-done.5
  141.3 2.3 %convolution_convert_fusion = bf16[256,2048]{1,0:T(8,128)(2,1)} fusion(bf16[1024,2048]{1,0:T(8,128)(2,1)S(1)} %copy-done.5, bf16[256,512]{1,0:T(8,128)(2,1)S(1)} %collective-permute-done.2, bf16[256,512]{1,0:T(8,128)(2,1)S(1)} %get-tuple-element.7, pred[]{:T(512)S(6)} %eq.2), kind=kOutput, calls=%fused_computation.2 | convolution fusion | flops 1076625408 | bytes 5767169 | tf_op jit(solution)/shard_map/dot_general | solution.py:197
  (11 shorter events, 0.2 us)
Async XLA Ops:
  6.5 3.8 %copy-start = (bf16[2048,128]{1,0:T(8,128)(2,1)S(1)}, bf16[2048,128]{1,0:T(8,128)(2,1)}, u32[]{:S(2)}) copy-start(bf16[2048,128]{1,0:T(8,128)(2,1)} %param.12) | copy-start | bytes 1572868
  6.5 3.8 %copy-start.2 = (bf16[256,2048]{1,0:T(8,128)(2,1)S(1)}, bf16[256,2048]{1,0:T(8,128)(2,1)}, u32[]{:S(2)}) copy-start(bf16[256,2048]{1,0:T(8,128)(2,1)} %param.9) | copy-start | bytes 3145732
  6.5 3.8 %copy-start.6 = (f32[2048]{0:T(1024)S(1)}, f32[2048]{0:T(1024)}, u32[]{:S(2)}) copy-start(f32[2048]{0:T(1024)} %param.10) | copy-start | bytes 24580
  6.5 63.6 %all-gather.3.cloned.1.call-start = ((), (), s32[]{:S(2)}) async-start(), calls=%async_computation | async-start | bytes 2646016 | tf_op jit(solution)/shard_map/all_gather | solution.py:154
  8.2 2.9 %copy-start.4 = (f32[64]{0:T(128)S(1)}, f32[64]{0:T(128)}, u32[]{:S(2)}) copy-start(f32[64]{0:T(128)} %param.15) | copy-start | bytes 772
  10.2 5.1 %copy-start.3 = (f32[1024,4]{0,1:T(4,128)S(1)}, f32[1024,4]{0,1:T(4,128)}, u32[]{:S(2)}) copy-start(f32[1024,4]{0,1:T(4,128)} %param.16) | copy-start | bytes 49156
  11.4 7.7 %collective-permute-start.1 = (bf16[256,128]{1,0:T(8,128)(2,1)S(1)}, bf16[256,128]{1,0:T(8,128)(2,1)S(1)}, u32[]{:S(2)}, u32[]{:S(2)}) collective-permute-start(bf16[256,128]{1,0:T(8,128)(2,1)S(1)} %select_bitcast_fusion.1), channel_id=1, source_target_pairs={{0,31},{1,30},{2,29},{3,28},{4,27},{5,26},{6,25},{7,24},{8,23},{9,... | collective-permute-start | bytes 196616 | tf_op jit(solution)/shard_map/ppermute | solution.py:146
  24.7 0.7 copy-start.7
  26.9 20.6 %collective-permute-start = (bf16[256,512]{1,0:T(8,128)(2,1)S(1)}, bf16[256,512]{1,0:T(8,128)(2,1)S(1)}, u32[]{:S(2)}, u32[]{:S(2)}) collective-permute-start(bf16[256,512]{1,0:T(8,128)(2,1)S(1)} %get-tuple-element.10), channel_id=1, source_target_pairs={{0,31},{1,30},{2,29},{3,28},{4,27},{5,26},{6,25},{7,24},{8,23},{9,... | collective-permute-start | bytes 786440 | tf_op jit(solution)/shard_map/ppermute | solution.py:163
  70.2 4.7 %copy-start.1 = (bf16[9728,128]{1,0:T(8,128)(2,1)S(1)}, bf16[9728,128]{1,0:T(8,128)(2,1)}, u32[]{:S(2)}) copy-start(bf16[9728,128]{1,0:T(8,128)(2,1)} %all-gather.3.cloned.1.call-done) | copy-start | bytes 7471108
  74.9 66.4 %copy-start.5 = (bf16[1024,2048]{1,0:T(8,128)(2,1)S(1)}, bf16[1024,2048]{1,0:T(8,128)(2,1)}, u32[]{:S(2)}) copy-start(bf16[1024,2048]{1,0:T(8,128)(2,1)} %param.17) | copy-start | bytes 12582916
  125.6 15.7 %collective-permute-start.2 = (bf16[256,512]{1,0:T(8,128)(2,1)S(1)}, bf16[256,512]{1,0:T(8,128)(2,1)S(1)}, u32[]{:S(2)}, u32[]{:S(2)}) collective-permute-start(bf16[256,512]{1,0:T(8,128)(2,1)S(1)} %get-tuple-element.8), channel_id=1, source_target_pairs={{0,31},{1,30},{2,29},{3,28},{4,27},{5,26},{6,25},{7,24},{8,23},{9,... | collective-permute-start | bytes 786440 | tf_op jit(solution)/shard_map/ppermute | solution.py:193
Sparse Core Ops, SparseCore 0:
  20.0 50.1 all-gather.2

commit v2 on v1

v2 whole, which is shorter than its diff:
```python
import math

import jax
import jax.numpy as jnp
from jax import lax
from jax.experimental import pallas as pl
from jax.experimental.pallas import tpu as pltpu
from jax.sharding import Mesh, PartitionSpec as P

epsilon = 1e-06
LOG2E = math.log2(math.e)
ALL = ("sp", "kv", "half")
HEADS_PER_DOT = 2
KEY_BLOCK = 512
SMALL = 60.0


def rms_norm(vector, gain_vec):
    return (
        vector * lax.rsqrt(jnp.mean(vector * vector, axis=-1, keepdims=True) + epsilon) * gain_vec
    )


def exchange_kernel(
    kv_ref, q_ref, decay_ref, kv_out, q_out, decay_out, own_sems, kv_send, kv_recv, kv_relay,
    decay_send, decay_recv, decay_relay, q_send, q_recv, *, rows, sizes
):
    sp_count, kv_heads, half_count = sizes
    sp, group, half = lax.axis_index("sp"), lax.axis_index("kv"), lax.axis_index("half")
    core, chips = half % 2, half_count // 2
    partner = (sp, group, half + 1 - 2 * core)

    def device_of(chip):
        return (chip // (kv_heads * chips), (chip // chips) % kv_heads, (chip % chips) * 2 + core)

    def block_of(place):
        return (place[0] * kv_heads + place[1]) * half_count + place[2]

    def kv_copy(source, block, send, device):
        return pltpu.make_async_remote_copy(
            src_ref=source, dst_ref=kv_out.at[pl.ds(pl.multiple_of(block * rows, rows), rows)],
            send_sem=send, recv_sem=kv_recv.at[block], device_id=device,
            device_id_type=pl.DeviceIdType.MESH,
        )

    def decay_copy(source, member, send, device):
        return pltpu.make_async_remote_copy(
            src_ref=source, dst_ref=decay_out.at[member], send_sem=send,
            recv_sem=decay_recv.at[member], device_id=device,
            device_id_type=pl.DeviceIdType.MESH,
        )

    me = block_of((sp, group, half))
    chip = (sp * kv_heads + group) * chips + half // 2
    total = sp_count * kv_heads * chips
    member = sp * half_count + half
    cluster = sp * chips + half // 2
    clusters = sp_count * chips
    started = []
    for k in range(1, total):
        place = device_of((chip + k) % total)
        started.append(kv_copy(kv_ref.at[place[1]], me, kv_send.at[k], place))
        started[-1].start()
    for k in range(1, clusters):
        other = (cluster + k) % clusters
        place = (other // chips, group, (other % chips) * 2 + core)
        started.append(decay_copy(decay_ref, member, decay_send.at[k], place))
        started[-1].start()
    q_copy = pltpu.make_async_remote_copy(
        src_ref=q_ref, dst_ref=q_out, send_sem=q_send, recv_sem=q_recv,
        device_id=(sp_count - 1 - sp, kv_heads - 1 - group, half_count - 1 - half),
        device_id_type=pl.DeviceIdType.MESH,
    )
    q_copy.start()
    started.append(kv_copy(kv_ref.at[group], me, kv_relay.at[0], partner))
    started[-1].start()
    started.append(decay_copy(decay_ref, member, decay_relay.at[0], partner))
    started[-1].start()
    own_kv = pltpu.make_async_copy(
        kv_ref.at[group], kv_out.at[pl.ds(pl.multiple_of(me * rows, rows), rows)], own_sems.at[0]
    )
    own_kv.start()
    own_decay = pltpu.make_async_copy(decay_ref, decay_out.at[member], own_sems.at[1])
    own_decay.start()
    for k in range(1, clusters):
        other = (cluster + clusters - k) % clusters
        which = (other // chips) * half_count + (other % chips) * 2 + core
        landed = decay_out.at[which]
        relay = decay_copy(landed, which, decay_relay.at[k], partner)
        relay.wait_recv()
        relay.start()
        started.append(relay)
    for k in range(1, total):
        block = block_of(device_of((chip + total - k) % total))
        landed = kv_out.at[pl.ds(pl.multiple_of(block * rows, rows), rows)]
        relay = kv_copy(landed, block, kv_relay.at[k], partner)
        relay.wait_recv()
        relay.start()
        started.append(relay)
    for k in range(clusters):
        other = (cluster + clusters - k) % clusters
        which = (other // chips) * half_count + (other % chips) * 2 + 1 - core
        decay_copy(decay_out.at[which], which, decay_relay.at[k], partner).wait_recv()
    for k in range(total):
        place = device_of((chip + total - k) % total)
        block = block_of((place[0], place[1], place[2] + 1 - 2 * core))
        landed = kv_out.at[pl.ds(pl.multiple_of(block * rows, rows), rows)]
        kv_copy(landed, block, kv_relay.at[k], partner).wait_recv()
    for copy in started:
        copy.wait_send()
    own_kv.wait()
    own_decay.wait()
    q_copy.wait()


def attend_kernel(
    place_ref, near_ref, far_ref, row_ref, decay_ref, kv_ref, out_ref, ones_ref, q_ref, peak_ref,
    acc_ref, *, rows, heads, key_block, small
):
    lane = lax.broadcasted_iota(jnp.int32, (rows, 128), 1)
    low = lane < 64
    for r, ref in enumerate((near_ref, far_ref)):
        for pair in range(heads // 2):
            both = ref[:, pair * 128 : (pair + 1) * 128].astype(jnp.float32)
            even = jnp.where(low, both, 0.0)
            odd = jnp.where(low, pltpu.roll(both, 64, 1), 0.0)
            q_ref[r, (2 * pair) * rows : (2 * pair + 1) * rows] = even.astype(jnp.bfloat16)
            q_ref[r, (2 * pair + 1) * rows : (2 * pair + 2) * rows] = odd.astype(jnp.bfloat16)

    def fill(i, carry):
        at = pl.ds(pl.multiple_of(i * key_block, key_block), key_block)
        wide = lax.broadcasted_iota(jnp.int32, (key_block, 128), 1) < 64
        ones_ref[at] = jnp.where(wide, 1.0, kv_ref[at].astype(jnp.float32)).astype(jnp.bfloat16)
        return carry

    lax.fori_loop(0, kv_ref.shape[0] // key_block, fill, 0)
    span = HEADS_PER_DOT * rows

    for r in range(2):
        first = place_ref[r]
        for head in range(heads):
            part = pl.ds(head * rows, rows)
            if small:
                peak_ref[part] = jnp.broadcast_to(row_ref[r, :, head : head + 1], (rows, 128))
            else:
                peak_ref[part] = jnp.full((rows, 128), -1e30, jnp.float32)
        acc_ref[...] = jnp.zeros_like(acc_ref)

        def step(index, masked):
            at = pl.ds(pl.multiple_of(index * key_block, key_block), key_block)
            keys = kv_ref[at]
            values = ones_ref[at]
            for start in range(0, heads, HEADS_PER_DOT):
                part = pl.ds(start * rows, span)
                before = peak_ref[part]
                scores = lax.dot_general(
                    q_ref[r, part], keys, (((1,), (1,)), ((), ())),
                    preferred_element_type=jnp.float32,
                )
                if small:
                    scores = scores + jnp.concatenate([before] * (key_block // 128), axis=1)
                scores = scores.reshape(HEADS_PER_DOT, rows, key_block)
                scores = scores - decay_ref[index, start : start + HEADS_PER_DOT][:, None, :]
                if masked:
                    row = first + lax.broadcasted_iota(jnp.int32, (rows, key_block), 0)
                    col = index * key_block + lax.broadcasted_iota(
                        jnp.int32, (rows, key_block), 1
                    )
                    scores = jnp.where((col <= row)[None], scores, -1e30)
                scores = scores.reshape(span, key_block)
                if small:
                    weights = jnp.exp2(scores).astype(jnp.bfloat16)
                    acc_ref[part] += jnp.dot(weights, values, preferred_element_type=jnp.float32)
                else:
                    after = jnp.maximum(before, jnp.max(scores, axis=1, keepdims=True))
                    weights = jnp.exp2(scores - after[:, :1]).astype(jnp.bfloat16)
                    acc_ref[part] = acc_ref[part] * jnp.exp2(before - after) + jnp.dot(
                        weights, values, preferred_element_type=jnp.float32
                    )
                    peak_ref[part] = after

        full = first // key_block

        def body(index, carry):
            step(index, False)
            return carry

        lax.fori_loop(0, full, body, 0)
        step(full, True)
        for pair in range(heads // 2):
            even = acc_ref[(2 * pair) * rows : (2 * pair + 1) * rows]
            odd = acc_ref[(2 * pair + 1) * rows : (2 * pair + 2) * rows]
            done = jnp.where(low, pltpu.roll(even, 64, 1), odd) / jnp.where(
                low, even, pltpu.roll(odd, 64, 1)
            )
            out_ref[r, :, pair * 128 : (pair + 1) * 128] = done.astype(jnp.bfloat16)


def attend(place, near, far, row_decay, decays, kv, small):
    length = kv.shape[0]
    rows, width = near.shape
    heads, key_block = decays.shape[1:]
    vmem = pl.BlockSpec(memory_space=pltpu.VMEM)
    return pl.pallas_call(
        lambda *refs: attend_kernel(
            *refs, rows=rows, heads=heads, key_block=key_block, small=small
        ),
        out_shape=jax.ShapeDtypeStruct((2, rows, width), jnp.bfloat16),
        in_specs=[pl.BlockSpec(memory_space=pltpu.SMEM)] + [vmem] * 5,
        out_specs=vmem,
        scratch_shapes=[
            pltpu.VMEM((length, 128), jnp.bfloat16),
            pltpu.VMEM((2, heads * rows, 128), jnp.bfloat16),
            pltpu.VMEM((heads * rows, 128), jnp.float32),
            pltpu.VMEM((heads * rows, 128), jnp.float32),
        ],
        compiler_params=pltpu.CompilerParams(vmem_limit_bytes=40 * 1024 * 1024),
        name="attend_small" if small else "attend_any",
    )(place, near, far, row_decay, decays, kv)


def per_device(inputs, in_gain, w_query, w_key, w_value, query_gain, key_gain, decay_sums, w_out):
    sp_count = lax.axis_size("sp")
    kv_heads = lax.axis_size("kv")
    half_count = lax.axis_size("half")
    tp_count = kv_heads * half_count
    group = lax.axis_index("kv")
    me = (lax.axis_index("sp") * kv_heads + group) * half_count + lax.axis_index("half")
    count = sp_count * tp_count
    mirror = [(i, count - 1 - i) for i in range(count)]
    head_size = query_gain.shape[0]
    rows = inputs.shape[0]
    length = rows * count
    all_heads = w_query.shape[1] // head_size
    heads = all_heads // kv_heads
    width = heads * head_size
    members = sp_count * half_count
    key_block = math.gcd(length, KEY_BLOCK)

    def choose(a, b):
        return jnp.where(group == 0, a, b)

    normed = rms_norm(inputs.astype(jnp.float32), in_gain).astype(jnp.bfloat16)
    keys = rms_norm(
        jnp.dot(normed, w_key, preferred_element_type=jnp.float32).reshape(
            rows, kv_heads, head_size
        ),
        key_gain,
    ).astype(jnp.bfloat16)
    values = (
        jnp.dot(normed, w_value, preferred_element_type=jnp.float32)
        .astype(jnp.bfloat16)
        .reshape(rows, kv_heads, head_size)
    )
    pairs = jnp.concatenate([keys, values], axis=2)
    kv_blocks = pairs.transpose(1, 0, 2)
    decay_rows = (decay_sums.T * LOG2E).reshape(-1, 128)

    queries = rms_norm(
        jnp.dot(normed, w_query, preferred_element_type=jnp.float32).reshape(
            rows, all_heads, head_size
        ),
        query_gain * (LOG2E * head_size ** (-0.5)),
    ).astype(jnp.bfloat16).reshape(rows, kv_heads * width)
    own_q = choose(queries[:, :width], queries[:, width:])
    sent_q = choose(queries[:, width:], queries[:, :width])
    vmem = pl.BlockSpec(memory_space=pltpu.VMEM)
    chips = count // 2
    dma = pltpu.SemaphoreType.DMA
    kv, far_q, decay_all = pl.pallas_call(
        lambda *refs: exchange_kernel(
            *refs, rows=rows, sizes=(sp_count, kv_heads, half_count)
        ),
        out_shape=(
            jax.ShapeDtypeStruct((length, 128), jnp.bfloat16),
            jax.ShapeDtypeStruct((rows, width), jnp.bfloat16),
            jax.ShapeDtypeStruct((members, *decay_rows.shape), jnp.float32),
        ),
        in_specs=[vmem] * 3,
        out_specs=(vmem,) * 3,
        scratch_shapes=[
            dma((2,)), dma((chips,)), dma((count,)), dma((chips,)), dma((members // 2,)),
            dma((members,)), dma((members // 2,)), dma, dma,
        ],
        compiler_params=pltpu.CompilerParams(has_side_effects=True),
        name="exchange",
    )(kv_blocks, sent_q, decay_rows)
    decay_all = decay_all.reshape(sp_count, heads, -1, key_block)
    decay_all = decay_all.transpose(0, 2, 1, 3).reshape(length // key_block, heads, key_block)
    firsts = (me * rows, (count - 1 - me) * rows)
    place = jnp.stack(firsts).astype(jnp.int32)
    row_decay = jnp.stack(
        [
            lax.dynamic_slice(
                decay_all, (first // key_block, 0, first % key_block), (1, heads, rows)
            )[0].T
            for first in firsts
        ]
    )
    bound = head_size**0.5 * LOG2E * jnp.max(query_gain) * jnp.max(key_gain)
    attended = lax.cond(
        bound <= SMALL,
        lambda *given: attend(*given, True),
        lambda *given: attend(*given, False),
        place, own_q, far_q, row_decay, decay_all, kv,
    )
    back = lax.ppermute(attended[1], ALL, mirror)
    whole = choose(
        jnp.concatenate([attended[0], back], axis=1), jnp.concatenate([back, attended[0]], axis=1)
    )
    return jnp.dot(whole, w_out, preferred_element_type=jnp.float32).astype(jnp.bfloat16)


def solution(mesh):
    sp_count, tp_count = mesh.devices.shape
    split = Mesh(mesh.devices.reshape(sp_count, 2, tp_count // 2), ALL)
    placed = (P(ALL, None), P(), P(), P(), P(), P(), P(), P("sp", ("kv", "half")), P())
    return jax.shard_map(
        per_device, mesh=split, in_specs=placed, out_specs=P(ALL, None), check_vma=False
    )
```

time: 151 us -> 140 us (0.927)
  Pallas kernels: 50.7 us -> 99.8 us
  waiting for transfers between devices: 58.6 us -> 13.4 us
  between operations: 13.6 us -> 1.47 us
  starting transfers between devices: 7.89 us -> 0.07 us
  other arithmetic: 5.12 us -> 9.2 us
  matrix products: 9.27 us -> 11.4 us
    pallas_call x1 -> x2, Pallas kernels: 50.7 us -> 99.8 us  [the longest x1 50.9 us: per_device(): pl.pallas_call(lambda *refs: exchange_kernel(*refs, rows=rows, sizes=(sp_...]
    all_gather x1 -> x0, waiting for transfers between devices: 22.7 us -> none  [per_device(): gathered = lax.all_gather(packed, ('sp', 'half'), axis=0, tiled=False)]
    ppermute x2 -> x0, waiting for transfers between devices: 22.1 us -> none  [the longest x1 18.2 us: per_device(): lax.ppermute(choose(queries[:, width:], queries[:, :width]), ALL, mirror)]
    ppermute x2 -> x0, starting transfers between devices: 6.12 us -> none  [the longest x1 3.81 us: per_device(): far_kv = lax.ppermute(choose(pairs[:, 1], pairs[:, 0]), ALL, mirror)]
    dot_general x1, matrix products: 2.26 us -> 4.43 us  [per_device(): jnp.dot(whole, w_out, preferred_element_type=jnp.float32)]
    ppermute x1, starting transfers between devices: 1.77 us -> 0.07 us  [per_device(): back = lax.ppermute(attended[1], ALL, mirror)]
  transfers between devices with their start and end apart: 4 -> 1, of which waited for: 4 -> 1; matrix products, arithmetic and copies ran while one was open for 5% -> 0% of each run, Pallas kernels for 0% -> 0%
where the time goes in v2:
time: 140 us; the launch traced here: 139 us
  Pallas kernels  99.8 us (71%)
  waiting for transfers between devices  13.4 us (10%)
  matrix products  11.4 us (8%)
  other arithmetic  9.2 us (7%)
  local copies, waits for them, and re-layouts  4.11 us (3%)
  between operations  1.47 us (1%)
    pallas_call x1, Pallas kernels, per_device(): pl.pallas_call(lambda *refs: exchange_kernel(*refs, rows=rows, sizes=(sp_...  50.9 us
    pallas_call x1, Pallas kernels, attend(): pl.pallas_call(lambda *refs: attend_kernel(*refs, rows=rows, heads=heads,...  48.8 us
    ppermute x1, waiting for transfers between devices, per_device(): back = lax.ppermute(attended[1], ALL, mirror)  13.4 us
    dot_general x1, matrix products, per_device(): jnp.dot(normed, w_query, preferred_element_type=jnp.float32)  4.46 us
    dot_general x1, matrix products, per_device(): jnp.dot(whole, w_out, preferred_element_type=jnp.float32)  4.43 us
  transfers between devices with their start and end apart: 1, of which 1 were waited for; matrix products, arithmetic and copies ran while one was open for 0% of the time, Pallas kernels for 0%

profile of v2, /device:TPU:9, one launch (start us, length us, event | category | flops | bytes accessed | tf_op | source)
XLA Modules:
  0.0 139.4 jit_solution(17819943625331422007)
XLA Ops:
  0.0 0.0 copy-start
  0.0 0.0 copy-start.1
  0.0 0.0 copy-start.3
  0.1 1.6 %fusion = f32[256]{0:T(256)S(1)} fusion(bf16[256,2048]{1,0:T(8,128)(2,1)} %param.11), kind=kLoop, calls=%fused_computation.5 | loop fusion | flops 1572608 | bytes 1049600 | tf_op jit(solution)/shard_map/reduce_sum | solution.py:20
  1.7 1.3 broadcast_multiply_fusion
  3.0 1.3 reduce_max.19
  5.4 0.1 mul.116
  5.5 0.7 multiply_bitcast_fusion
  6.2 0.6 reshape.49.refs_2_
  6.9 1.9 %convolution_convert_fusion.1 = bf16[256,128]{0,1:T(8,128)(2,1)S(1)} fusion(bf16[2048,128]{1,0:T(8,128)(2,1)} %param.15, bf16[256,2048]{1,0:T(8,128)(2,1)} %param.11, f32[2048]{0:T(1024)} %param.12, f32[256]{0:T(256)S(1)} %add_rsqrt_fusion.2), kind=kOutput, calls=%fused_computation.8 | convolution fusion | flops 136347648 | bytes 1647616 | tf_op jit(solution)/shard_map/dot_general | solution.py:251
  8.8 0.1 copy.12
  8.9 0.0 copy-done
  8.9 0.0 copy-done.1
  9.0 0.0 copy-done.3
  9.0 0.6 multiply_reduce_fusion
  9.6 0.1 copy.11
  9.7 4.5 %fusion.16 = (f32[256,1024]{1,0:T(8,128)S(1)}, f32[256,1024]{1,0:T(8,128)}) fusion(bf16[2048,1024]{1,0:T(8,128)(2,1)} %param.13, bf16[256,2048]{1,0:T(8,128)(2,1)S(1)} %copy-done.1, f32[2048]{0:T(1024)S(1)} %copy-done.3, f32[256]{0:T(256)S(1)} %add_rsqrt_fusion.2), kind=kOutput, calls=%fused_computation.37 | convolution fusion | flops 1076101120 | bytes 7349248 | tf_op jit(solution)/shard_map/dot_general | solution.py:260
  14.2 0.3 copy.13
  14.5 0.0 copy-start.2
  14.5 0.1 bitcast_reduce_fusion
  14.6 0.1 mul.110
  14.7 0.3 copy.14
  15.0 0.1 copy-done.2
  15.2 0.1 multiply_convert_fusion.1
  15.3 0.8 maximum_bitcast_fusion.refs_0_
  16.1 1.4 %multiply_convert_fusion = bf16[256,1024]{1,0:T(8,128)(2,1)S(1)} fusion(f32[256,1024]{1,0:T(8,128)} %get-tuple-element.84, f32[256,1024]{1,0:T(8,128)S(1)} %copy.14, f32[1024]{0:T(1024)S(1)} %mul.116), kind=kLoop, calls=%fused_computation.10 | loop fusion | flops 786432 | bytes 2625536 | tf_op jit(solution)/shard_map/convert_element_type | solution.py:264
  17.5 0.8 fusion.15
  18.3 50.9 %exchange.1 = (bf16[8192,128]{1,0:T(8,128)(2,1)S(1)}, bf16[256,512]{1,0:T(8,128)(2,1)}, f32[16,32,128]{2,1,0:T(8,128)}) custom-call(bf16[2,256,128]{2,1,0:T(8,128)(2,1)} %maximum_bitcast_fusion.refs_0_, bf16[256,512]{1,0:T(8,128)(2,1)} %get-tuple-element.77.refs_1_, f32[32,128]{1,0:T(8,128)} %reshape.49.refs_2_), custom_call_target="tpu_custom_call" | custom-call | tf_op jit(solution)/shard_map/exchange/pallas_call | solution.py:270
  69.3 1.1 reshape.50
  70.4 0.1 pad_add_fusion
  70.5 49.9 %conditional.1 = (bf16[2,256,512]{2,1,0:T(8,128)(2,1)}) conditional(s32[]{:T(128)} %convert_element_type.22, (s32[2]{0:T(128)S(1)}, pred[]{:T(512)}, bf16[256,512]{1,0:T(8,128)(2,1)}, f32[2,256,8]{1,2,0:T(8,128)S(1)}, f32[16,8,512]{2,1,0:T(8,128)S(1)}, /*index=5*/bf16[8192,128]{1,0:T(8,128)(2,1)S(1)}, bf16[256,512]{1,0:T(8,128)(2,1)}, ...), branch_computations={%region_5.6_spmd, %region_6.7_spmd} | conditional | flops 131072 | bytes 819209 | solution.py:301
  70.5 1.0 broadcast_select_fusion.refs_1_
  71.5 0.1 copy.16.refs_3_
  71.6 48.8 %attend_any.1 = bf16[2,256,512]{2,1,0:T(8,128)(2,1)} custom-call(s32[2]{0:T(128)S(1)} %get-tuple-element.32.refs_0_, bf16[256,512]{1,0:T(8,128)(2,1)S(1)} %broadcast_select_fusion.refs_1_, bf16[256,512]{1,0:T(8,128)(2,1)} %get-tuple-element.34.refs_2_, f32[2,256,8]{2,1,0:T(8,128)S(1)} %copy.16.refs_3_, f32[16,8,512]{2,1,0:T(8,128)S(1)} %get-tuple-element.36.refs_4_, ...), custom_call_target="tpu_custom_call" | custom-call | tf_op jit(solution)/shard_map/cond/branch_0_fun/attend_any/pallas_call | solution.py:204
  120.5 1.1 slice_bitcast_fusion.1
  121.5 0.1 collective-permute-start
  121.6 13.4 %collective-permute-done = bf16[256,512]{1,0:T(8,128)(2,1)S(1)} collective-permute-done((bf16[256,512]{1,0:T(8,128)(2,1)S(1)}, bf16[256,512]{1,0:T(8,128)(2,1)S(1)}, u32[]{:S(2)}, u32[]{:S(2)}) %collective-permute-start) | collective-permute-done | bytes 262176 | tf_op jit(solution)/shard_map/ppermute | solution.py:307
  135.0 4.4 %convolution_convert_fusion = bf16[256,2048]{1,0:T(8,128)(2,1)} fusion(bf16[1024,2048]{1,0:T(8,128)(2,1)} %param.19, bf16[256,512]{1,0:T(8,128)(2,1)S(1)} %collective-permute-done, bf16[256,512]{1,0:T(8,128)(2,1)S(1)} %get-tuple-element.74, pred[]{:T(512)} %eq.8), kind=kOutput, calls=%fused_computation.4 | convolution fusion | flops 1076625408 | bytes 5767169 | tf_op jit(solution)/shard_map/dot_general | solution.py:311
  (7 shorter events, 0.1 us)
Async XLA Ops:
  0.0 8.9 %copy-start = (bf16[2048,128]{1,0:T(8,128)(2,1)S(1)}, bf16[2048,128]{1,0:T(8,128)(2,1)}, u32[]{:S(2)}) copy-start(bf16[2048,128]{1,0:T(8,128)(2,1)} %param.14) | copy-start | bytes 1572868
  0.0 8.9 %copy-start.1 = (bf16[256,2048]{1,0:T(8,128)(2,1)S(1)}, bf16[256,2048]{1,0:T(8,128)(2,1)}, u32[]{:S(2)}) copy-start(bf16[256,2048]{1,0:T(8,128)(2,1)} %param.11) | copy-start | bytes 3145732
  0.0 8.9 %copy-start.3 = (f32[2048]{0:T(1024)S(1)}, f32[2048]{0:T(1024)}, u32[]{:S(2)}) copy-start(f32[2048]{0:T(1024)} %param.12) | copy-start | bytes 24580
  14.5 0.7 copy-start.2
  121.5 13.5 %collective-permute-start = (bf16[256,512]{1,0:T(8,128)(2,1)S(1)}, bf16[256,512]{1,0:T(8,128)(2,1)S(1)}, u32[]{:S(2)}, u32[]{:S(2)}) collective-permute-start(bf16[256,512]{1,0:T(8,128)(2,1)S(1)} %get-tuple-element.75), channel_id=1, source_target_pairs={{0,31},{1,30},{2,29},{3,28},{4,27},{5,26},{6,25},{7,24},{8,23},{9,... | collective-permute-start | bytes 786440 | tf_op jit(solution)/shard_map/ppermute | solution.py:307

commit v3 on v2

--- a/solution.py
+++ b/solution.py
@@ -297,16 +297,23 @@
             for first in firsts
         ]
     )
-    bound = head_size**0.5 * LOG2E * jnp.max(query_gain) * jnp.max(key_gain)
-    attended = lax.cond(
-        bound <= SMALL,
-        lambda *given: attend(*given, True),
-        lambda *given: attend(*given, False),
-        place, own_q, far_q, row_decay, decay_all, kv,
-    )
-    back = lax.ppermute(attended[1], ALL, mirror)
+    bound = head_size**0.5 * LOG2E * jnp.max(query_gain[:, None] * key_gain)
+    near, far = [], []
+    step = heads // 2 if heads % 4 == 0 else heads
+    for start in range(0, heads, step):
+        cols = slice(start * head_size, (start + step) * head_size)
+        some = slice(start, start + step)
+        attended = lax.cond(
+            bound <= SMALL,
+            lambda *given: attend(*given, True),
+            lambda *given: attend(*given, False),
+            place, own_q[:, cols], far_q[:, cols], row_decay[:, :, some], decay_all[:, some], kv,
+        )
+        near.append(attended[0])
+        far.append(lax.ppermute(attended[1], ALL, mirror))
+    near, back = jnp.concatenate(near, axis=1), jnp.concatenate(far, axis=1)
     whole = choose(
-        jnp.concatenate([attended[0], back], axis=1), jnp.concatenate([back, attended[0]], axis=1)
+        jnp.concatenate([near, back], axis=1), jnp.concatenate([back, near], axis=1)
     )
     return jnp.dot(whole, w_out, preferred_element_type=jnp.float32).astype(jnp.bfloat16)
 

time: 140 us -> 146 us (1.043)
  waiting for transfers between devices: 13.4 us -> 6.08 us
  Pallas kernels: 99.8 us -> 106 us
  local copies, waits for them, and re-layouts: 4.11 us -> 8.55 us
  starting transfers between devices: 0.07 us -> 3.71 us
    ppermute x1 -> x2, waiting for transfers between devices: 13.4 us -> 6.08 us  [per_device(): far.append(lax.ppermute(attended[1], ALL, mirror))]
    pallas_call x1 -> x2, Pallas kernels: 48.8 us -> 54.9 us  [attend(): pl.pallas_call(lambda *refs: attend_kernel(*refs, rows=rows, heads=heads,...]
    ppermute x1 -> x2, starting transfers between devices: 0.07 us -> 3.71 us  [per_device(): far.append(lax.ppermute(attended[1], ALL, mirror))]
    slice x0 -> x7, local copies, waits for them, and re-layouts: none -> 2.97 us  [the longest x2 1.83 us: per_device(): far_q[:, cols]]
  transfers between devices with their start and end apart: 1 -> 2, of which waited for: 1 -> 1; matrix products, arithmetic and copies ran while one was open for 0% -> 1% of each run, Pallas kernels for 0% -> 19%
where the time goes in v3:
time: 146 us; the launch traced here: 145 us
  Pallas kernels  106 us (73%)
  matrix products  11.7 us (8%)
  local copies, waits for them, and re-layouts  8.55 us (6%)
  other arithmetic  8.16 us (6%)
  waiting for transfers between devices  6.08 us (4%)
  starting transfers between devices  3.71 us (3%)
    pallas_call x2, Pallas kernels, attend(): pl.pallas_call(lambda *refs: attend_kernel(*refs, rows=rows, heads=heads,...  54.9 us
    pallas_call x1, Pallas kernels, per_device(): pl.pallas_call(lambda *refs: exchange_kernel(*refs, rows=rows, sizes=(sp_...  50.9 us
    ppermute x2, waiting for transfers between devices, per_device(): far.append(lax.ppermute(attended[1], ALL, mirror))  6.08 us
    dot_general x1, matrix products, per_device(): jnp.dot(whole, w_out, preferred_element_type=jnp.float32)  4.7 us
    dot_general x1, matrix products, per_device(): jnp.dot(normed, w_query, preferred_element_type=jnp.float32)  4.46 us
    ppermute x2, starting transfers between devices, per_device(): far.append(lax.ppermute(attended[1], ALL, mirror))  3.71 us
  transfers between devices with their start and end apart: 2, of which 1 were waited for; matrix products, arithmetic and copies ran while one was open for 1% of the time, Pallas kernels for 19%

profile of v3, /device:TPU:9, one launch (start us, length us, event | category | flops | bytes accessed | tf_op | source)
XLA Modules:
  0.0 145.0 jit_solution(12938471238792253348)
XLA Ops:
  0.0 0.0 copy-start
  0.0 0.0 copy-start.1
  0.0 0.0 copy-start.3
  0.1 0.8 broadcast_multiply_fusion
  0.8 1.4 multiply_reduce_fusion.1
  2.8 1.5 %fusion = f32[256]{0:T(256)S(1)} fusion(bf16[256,2048]{1,0:T(8,128)(2,1)} %param.13), kind=kLoop, calls=%fused_computation.3 | loop fusion | flops 1572608 | bytes 1049600 | tf_op jit(solution)/shard_map/reduce_sum | solution.py:20
  4.4 0.1 mul.128
  4.5 0.7 multiply_bitcast_fusion
  5.2 0.6 reshape.51.refs_2_
  5.8 1.9 %convolution_convert_fusion.1 = bf16[256,128]{0,1:T(8,128)(2,1)S(1)} fusion(bf16[2048,128]{1,0:T(8,128)(2,1)} %param.17, bf16[256,2048]{1,0:T(8,128)(2,1)} %param.13, f32[2048]{0:T(1024)} %param.14, f32[256]{0:T(256)S(1)} %add_rsqrt_fusion.2), kind=kOutput, calls=%fused_computation.6 | convolution fusion | flops 136347648 | bytes 1647616 | tf_op jit(solution)/shard_map/dot_general | solution.py:251
  7.7 0.1 copy.23
  7.9 0.0 copy-done
  7.9 0.0 copy-done.1
  7.9 0.0 copy-done.3
  7.9 0.6 multiply_reduce_fusion
  8.5 0.1 copy.22
  8.6 4.5 %fusion.23 = (f32[256,1024]{1,0:T(8,128)S(1)}, f32[256,1024]{1,0:T(8,128)}) fusion(bf16[2048,1024]{1,0:T(8,128)(2,1)} %param.15, bf16[256,2048]{1,0:T(8,128)(2,1)S(1)} %copy-done.1, f32[2048]{0:T(1024)S(1)} %copy-done.3, f32[256]{0:T(256)S(1)} %add_rsqrt_fusion.2), kind=kOutput, calls=%fused_computation.46 | convolution fusion | flops 1076101120 | bytes 7349248 | tf_op jit(solution)/shard_map/dot_general | solution.py:260
  13.1 0.3 copy.20
  13.4 0.0 copy-start.2
  13.4 0.1 bitcast_reduce_fusion
  13.6 0.1 mul.122
  13.6 0.3 copy.21
  14.0 0.1 copy-done.2
  14.1 0.1 multiply_convert_fusion.1
  14.2 0.7 maximum_bitcast_fusion.refs_0_
  15.0 1.4 multiply_convert_fusion
  16.4 0.7 broadcast_select_fusion
  17.1 50.9 %exchange.1 = (bf16[8192,128]{1,0:T(8,128)(2,1)S(1)}, bf16[256,512]{1,0:T(8,128)(2,1)}, f32[16,32,128]{2,1,0:T(8,128)}) custom-call(bf16[2,256,128]{2,1,0:T(8,128)(2,1)} %maximum_bitcast_fusion.refs_0_, bf16[256,512]{1,0:T(8,128)(2,1)} %get-tuple-element.153.refs_1_, f32[32,128]{1,0:T(8,128)} %reshape.51.refs_2_), custom_call_target="tpu_custom_call" | custom-call | tf_op jit(solution)/shard_map/exchange/pallas_call | solution.py:270
  68.1 1.1 reshape.52
  69.2 0.7 pad_add_fusion
  69.9 30.7 %conditional.3 = (bf16[2,256,256]{2,1,0:T(8,128)(2,1)}) conditional(s32[]{:T(128)} %convert_element_type.23, (s32[2]{0:T(128)}, bf16[256,512]{1,0:T(8,128)(2,1)S(1)}, bf16[256,512]{1,0:T(8,128)(2,1)}, f32[2,256,8]{1,2,0:T(8,128)S(1)}, f32[16,8,512]{2,1,0:T(8,128)S(1)}, /*index=5*/bf16[8192,128]{1,0:T(8,128)(2,1)S(1)}) %tuple.37, (s32[2]{0:T(128)}, ...), branch_computations={%region_6.7_spmd, %region_7.8_spmd} | conditional | bytes 835592 | solution.py:306
  69.9 0.9 slice.68.refs_2_
  70.9 0.8 copy.27
  71.7 1.1 slice.76.refs_3_
  72.8 27.8 %attend_any.3 = bf16[2,256,256]{2,1,0:T(8,128)(2,1)} custom-call(s32[2]{0:T(128)} %get-tuple-element.71.refs_0_, bf16[256,256]{1,0:T(8,128)(2,1)S(1)} %slice.66.refs_1_, bf16[256,256]{1,0:T(8,128)(2,1)S(1)} %slice.68.refs_2_, f32[2,256,4]{2,1,0:T(8,128)S(1)} %slice.76.refs_3_, f32[16,4,512]{2,1,0:T(4,128)S(1)} %slice.72.refs_4_, ...), custom_call_target="tpu_custom_call" | custom-call | tf_op jit(solution)/shard_map/cond/branch_0_fun/attend_any/pallas_call | solution.py:204
  100.6 1.7 %slice_bitcast_fusion.2 = (bf16[256,256]{1,0:T(8,128)(2,1)}, bf16[256,256]{1,0:T(8,128)(2,1)}) fusion(bf16[2,256,256]{2,1,0:T(8,128)(2,1)} %get-tuple-element.166), kind=kLoop, calls=%fused_computation.29 | loop fusion | bytes 524288 | tf_op jit(solution)/shard_map/squeeze | solution.py:312
  102.3 0.0 collective-permute-start.1
  102.3 28.2 %conditional.2 = (bf16[2,256,256]{2,1,0:T(8,128)(2,1)S(1)}) conditional(s32[]{:T(128)} %convert_element_type.23, (s32[2]{0:T(128)}, bf16[256,512]{1,0:T(8,128)(2,1)S(1)}, bf16[256,512]{1,0:T(8,128)(2,1)}, f32[2,256,8]{1,2,0:T(8,128)S(1)}, f32[16,8,512]{2,1,0:T(8,128)S(1)}, /*index=5*/bf16[8192,128]{1,0:T(8,128)(2,1)S(1)}) %tuple.39, (s32[2]{0:T(128)}, ...), branch_computations={%region_4.5_spmd, %region_5.6_spmd} | conditional | bytes 819208 | solution.py:306
  102.3 0.9 slice.60.refs_2_
  103.2 0.1 copy.25
  103.4 27.1 %attend_any.2 = bf16[2,256,256]{2,1,0:T(8,128)(2,1)S(1)} custom-call(s32[2]{0:T(128)} %get-tuple-element.58.refs_0_, bf16[256,256]{1,0:T(8,128)(2,1)S(1)} %slice.58.refs_1_, bf16[256,256]{1,0:T(8,128)(2,1)S(1)} %slice.60.refs_2_, f32[2,256,4]{2,1,0:T(8,128)S(1)} %bitcast.40, f32[16,4,512]{2,1,0:T(4,128)S(1)} %slice.64.refs_4_, ...), custom_call_target="tpu_custom_call" | custom-call | tf_op jit(solution)/shard_map/cond/branch_0_fun/attend_any/pallas_call | solution.py:204
  130.5 3.7 %collective-permute-start = (bf16[256,256]{1,0:T(8,128)(2,1)S(1)}, bf16[256,256]{1,0:T(8,128)(2,1)S(1)}, u32[]{:S(2)}, u32[]{:S(2)}) collective-permute-start(bf16[256,256]{1,0:T(8,128)(2,1)S(1)} %get-tuple-element.156), channel_id=1, source_target_pairs={{0,31},{1,30},{2,29},{3,28},{4,27},{5,26},{6,25},{7,24},{8,23},{9,... | collective-permute-start | bytes 393224 | tf_op jit(solution)/shard_map/ppermute | solution.py:313
  134.2 0.0 collective-permute-done.1
  134.2 6.1 %collective-permute-done = bf16[256,256]{1,0:T(8,128)(2,1)S(1)} collective-permute-done((bf16[256,256]{1,0:T(8,128)(2,1)S(1)}, bf16[256,256]{1,0:T(8,128)(2,1)S(1)}, u32[]{:S(2)}, u32[]{:S(2)}) %collective-permute-start) | collective-permute-done | bytes 131104 | tf_op jit(solution)/shard_map/ppermute | solution.py:313
  140.3 4.7 %convolution_convert_fusion = bf16[256,2048]{1,0:T(8,128)(2,1)} fusion(bf16[1024,2048]{1,0:T(8,128)(2,1)} %param.21, bf16[256,256]{1,0:T(8,128)(2,1)} %collective-permute-done.1, bf16[256,256]{1,0:T(8,128)(2,1)S(1)} %collective-permute-done, bf16[256,256]{1,0:T(8,128)(2,1)} %get-tuple-element.157, bf16[256,256]{1,0:T(8,128)(2,1)S(1)} %get-tuple-element.155, ...), kind=kOutput, calls=%fused_computation.2 | convolution fusion | flops 1078722560 | bytes 5767169 | tf_op jit(solution)/shard_map/dot_general | solution.py:318
  (12 shorter events, 0.2 us)
Async XLA Ops:
  0.0 7.9 %copy-start = (bf16[2048,128]{1,0:T(8,128)(2,1)S(1)}, bf16[2048,128]{1,0:T(8,128)(2,1)}, u32[]{:S(2)}) copy-start(bf16[2048,128]{1,0:T(8,128)(2,1)} %param.16) | copy-start | bytes 1572868
  0.0 7.9 %copy-start.1 = (bf16[256,2048]{1,0:T(8,128)(2,1)S(1)}, bf16[256,2048]{1,0:T(8,128)(2,1)}, u32[]{:S(2)}) copy-start(bf16[256,2048]{1,0:T(8,128)(2,1)} %param.13) | copy-start | bytes 3145732
  0.0 7.9 %copy-start.3 = (f32[2048]{0:T(1024)S(1)}, f32[2048]{0:T(1024)}, u32[]{:S(2)}) copy-start(f32[2048]{0:T(1024)} %param.14) | copy-start | bytes 24580
  13.4 0.7 copy-start.2
  102.3 31.9 %collective-permute-start.1 = (bf16[256,256]{1,0:T(8,128)(2,1)}, bf16[256,256]{1,0:T(8,128)(2,1)}, u32[]{:S(2)}, u32[]{:S(2)}) collective-permute-start(bf16[256,256]{1,0:T(8,128)(2,1)} %get-tuple-element.158), channel_id=1, source_target_pairs={{0,31},{1,30},{2,29},{3,28},{4,27},{5,26},{6,25},{7,24},{8,23},{9,... | collective-permute-start | bytes 393224 | tf_op jit(solution)/shard_map/ppermute | solution.py:313
  130.5 9.8 %collective-permute-start = (bf16[256,256]{1,0:T(8,128)(2,1)S(1)}, bf16[256,256]{1,0:T(8,128)(2,1)S(1)}, u32[]{:S(2)}, u32[]{:S(2)}) collective-permute-start(bf16[256,256]{1,0:T(8,128)(2,1)S(1)} %get-tuple-element.156), channel_id=1, source_target_pairs={{0,31},{1,30},{2,29},{3,28},{4,27},{5,26},{6,25},{7,24},{8,23},{9,... | collective-permute-start | bytes 393224 | tf_op jit(solution)/shard_map/ppermute | solution.py:313
